TPU v7x, 32 devices: a whole 2x2x4 slice. The times are simulated.
32 devices in a mesh: ep: 16 (over z, y, x), tp: 2 (over core).
Axes of the slice: x: 2, y: 2, z: 4, core: 2. Of those that a mesh axis runs over, the one named last changes fastest.
Arguments:
- tokens: bfloat16 [2048, 2048], P('ep'), may hold values from -6 to 6
- cotangent: bfloat16 [2048, 2048], P('ep'), may hold values from -0.625 to 0.625
- routes: int32 [2048, 2], P('ep'), may hold values from 0 to 15, as said below
- router_group: bfloat16 [2048, 4], replicated, may hold values from -0.125 to 0.125
- router_expert: bfloat16 [2048, 16], replicated, may hold values from -0.125 to 0.125
- gate_proj: bfloat16 [16, 2048, 512], P('ep', None, 'tp'), may hold values from -0.125 to 0.125
- up_proj: bfloat16 [16, 2048, 512], P('ep', None, 'tp'), may hold values from -0.125 to 0.125
- down_proj: bfloat16 [16, 512, 2048], P('ep', 'tp'), may hold values from -0.25 to 0.25
Outputs:
- token_grad: bfloat16 [2048, 2048], P('ep', 'tp')
- gate_grad: bfloat16 [16, 2048, 512], P('ep', None, 'tp')
- up_grad: bfloat16 [16, 2048, 512], P('ep', None, 'tp')
- down_grad: bfloat16 [16, 512, 2048], P('ep', 'tp')
- gate_rows: float32 [16, 2048], P('ep')
- up_rows: float32 [16, 2048], P('ep')
- down_rows: float32 [16, 512], P('ep', 'tp')
- router_expert_grad: float32 [2048, 16], P(('ep', 'tp'))
- router_group_grad: float32 [2048, 4], P(('ep', 'tp'))
- router_rows: float32 [2048], P(('ep', 'tp'))
Inputs may be any that keep to these rules, and one draw needn't show every extreme that they name: `routes`: the 2 entries of a row are different experts of one group: their quotients by 4 are equal. Among the rows of one device no expert is named more than 32 times, and the experts of one group, the same for all devices, are each named exactly 32 times by the rows of every device.
All inputs are finite; a program needn't handle non-finite values.
Results may differ from a plain program's by a relative error of at most 0.014.
Values may be sent and summed in bfloat16 or wider, within the bound.
A program may use at most 64 MiB of HBM per device.

v0:
```python
import functools

import jax
import jax.numpy as jnp
from jax import lax
from jax.experimental import pallas as pl
from jax.experimental.pallas import tpu as pltpu
from jax.sharding import PartitionSpec as P

MESH = pl.DeviceIdType.MESH
BF = jnp.bfloat16
F32 = jnp.float32


def mm(a, b, da=1, db=0):
    return lax.dot_general(a, b, (((da,), (db,)), ((), ())), preferred_element_type=F32)


def lanes_of(shape, dim=1):
    return lax.broadcasted_iota(jnp.int32, shape, dim)


class Sizes:
    pass


def sizes_of(mesh, tokens, routes, router_group, router_expert, gate_proj):
    z = Sizes()
    z.n_ep, z.n_tp = mesh["ep"], mesh["tp"]
    z.rows, z.width = tokens.shape
    z.top = routes.shape[1]
    z.groups, z.experts = router_group.shape[1], router_expert.shape[1]
    z.gs = z.experts // z.groups
    z.cap = z.rows // z.gs
    z.gr = z.gs * z.cap // z.top
    z.r1 = z.groups * z.gr
    z.sl = z.groups * z.cap
    z.pairs = z.gs * z.sl
    z.ff = gate_proj.shape[2]
    z.cw = z.width // z.n_tp
    z.half_chunks = 4
    z.nc = 2 * z.half_chunks
    z.cc = z.cw // z.half_chunks
    z.rl = -(-(z.experts + z.groups) // 128) * 128
    z.rw = -(-(z.experts + z.groups) // 8) * 8
    z.ch = z.width // z.n_ep
    z.reduce_here = z.ch % 128 == 0 and z.n_ep % 2 == 0
    assert z.experts == z.n_ep and z.n_tp == 2 and z.top == 2
    assert z.sl & (z.sl - 1) == 0 and z.gr & (z.gr - 1) == 0
    return z


def kernel(
    z, tok_ref, cot_ref, routes_ref, rexp_ref, rgrp_ref, gate_ref, up_ref, down_ref,
    tg_out, gate_out, up_out, down_out, gsq_out, usq_out, dsq_out, rout_out,
    rc_ref, s1w, r1w,
    s_mat, t_mat, s1m, r1m, s1, r1, s2m, x2m, s2, x2, y2m, y2,
    gacc, uacc, pacc, dcat, hid, wcol, wp, wpr, pts, ptr, pto,
    s3m, r3m, s3, r3, s4m, r4m, s4, r4, sq, sqr, term, trec, tsum, tsumr,
    z1s, z1r, p2s, p2r, fs, fr, ptsm, ptrm, r3s, r3r, r4s, r4r, ms, mr, ts, tr,
):
    e, t = lax.axis_index("ep"), lax.axis_index("tp")
    g, p = e // z.gs, e % z.gs
    other = 1 - t

    def rcopy(src, dst, ss, rs, ep, tp):
        return pltpu.make_async_remote_copy(
            src_ref=src, dst_ref=dst, send_sem=ss, recv_sem=rs,
            device_id=(ep, tp), device_id_type=MESH,
        )

    barrier = pltpu.get_barrier_semaphore()
    for d in range(1, z.n_ep):
        pl.semaphore_signal(
            barrier, inc=1, device_id=((e + d) % z.n_ep, t), device_id_type=MESH
        )
    pl.semaphore_signal(barrier, inc=1, device_id=(e, other), device_id_type=MESH)

    sends = []

    def grows(h):
        return pl.ds(pl.multiple_of(h * z.gr, z.gr), z.gr)

    def prows(q):
        return pl.ds(pl.multiple_of(q * z.sl, z.sl), z.sl)

    def group_send(src, dst, ss, rs, c):
        for d in range(1, z.groups):
            h = (g + d) % z.groups
            cp = rcopy(src.at[grows(h)], dst.at[grows(g)], ss.at[c, d], rs.at[c, d], h * z.gs + p, t)
            cp.start()
            sends.append(cp)
        dst[grows(g), :] = src[grows(g), :]

    def group_wait(src, dst, ss, rs, c):
        for d in range(1, z.groups):
            h = (g + z.groups - d) % z.groups
            rcopy(src.at[grows(h)], dst.at[grows(h)], ss.at[c, d], rs.at[c, d], h * z.gs + p, t).wait_recv()

    def plane_send(src, dst, ss, rs, c):
        for d in range(1, z.gs):
            q = (p + d) % z.gs
            cp = rcopy(src.at[prows(q)], dst.at[prows(p)], ss.at[c, d], rs.at[c, d], g * z.gs + q, t)
            cp.start()
            sends.append(cp)
        dst[prows(p), :] = src[prows(p), :]

    def plane_wait_one(src, dst, ss, rs, c, d):
        q = (p + z.gs - d) % z.gs
        rcopy(src.at[prows(q)], dst.at[prows(q)], ss.at[c, d], rs.at[c, d], g * z.gs + q, t).wait_recv()

    def plane_wait(src, dst, ss, rs, c):
        for d in range(1, z.gs):
            plane_wait_one(src, dst, ss, rs, c, d)

    def pair_send(src, dst, ss, rs):
        cp = rcopy(src, dst, ss, rs, e, other)
        cp.start()
        sends.append(cp)
        return cp

    lane = lanes_of((z.rows, z.rl))
    eye = lanes_of((z.rows, z.rows), 0) == lanes_of((z.rows, z.rows), 1)

    def column(row):
        return jnp.sum(jnp.where(eye, row.astype(F32), 0.0), axis=1, keepdims=True).astype(jnp.int32)

    r0, r1_ = column(routes_ref[0:1, :]), column(routes_ref[1:2, :])
    chosen = (lane == r0) | (lane == r1_)
    low = (lane - z.experts) * z.gs
    is_group = (lane >= z.experts) & (lane < z.experts + z.groups)
    in_group = is_group & (r0 >= low) & (r0 < low + z.gs)

    def before(n):
        return (lanes_of((n, n), 1) < lanes_of((n, n), 0)).astype(F32).astype(BF)

    ghot = in_group.astype(F32)
    grank = mm(before(z.rows), ghot.astype(BF))
    grank = jnp.where(in_group, grank, -1.0).astype(BF)
    er, el = lanes_of((z.rl, z.r1), 0) - z.experts, lanes_of((z.rl, z.r1), 1)
    expand = ((el >= er * z.gr) & (el < (er + 1) * z.gr)).astype(F32).astype(BF)
    place = (lanes_of((z.rows, z.r1)) & (z.gr - 1)).astype(F32)
    s_mat[...] = (mm(grank, expand) == place).astype(F32).astype(BF)

    s1m[...] = mm(s_mat[...], chosen.astype(F32).astype(BF), 0, 0).astype(BF)
    pl.semaphore_wait(barrier, z.n_ep)
    group_send(s1m, r1m, z1s, z1r, z.nc)

    def cols_at(half, k):
        return pl.ds(pl.multiple_of(half * z.cw + k * z.cc, z.cc), z.cc)

    for c in range(z.nc):
        src = tok_ref if c < z.half_chunks else cot_ref
        s1[c] = mm(s_mat[...], src[:, cols_at(t, c % z.half_chunks)], 0, 0).astype(BF)
        group_send(s1.at[c], r1.at[c], z1s, z1r, c)

    rc_ref[...] = jnp.zeros_like(rc_ref)
    rc_ref[0 : z.experts, :] = rexp_ref[...]
    rc_ref[z.experts : z.experts + z.groups, :] = rgrp_ref[...]
    expd = jnp.exp(mm(tok_ref[...], rc_ref[...], 1, 1))
    gexp = jnp.where(is_group, expd, 0.0)
    gprob = gexp / jnp.sum(gexp, axis=1, keepdims=True)
    picked = jnp.sum(jnp.where(in_group, gprob, 0.0), axis=1, keepdims=True)
    pexp = jnp.where(chosen, expd, 0.0)
    paired = pexp / jnp.sum(pexp, axis=1, keepdims=True)
    s1w[...] = mm(s_mat[...], (picked * paired).astype(BF), 0, 0).astype(BF)
    group_send(s1w, r1w, z1s, z1r, z.nc + 1)

    group_wait(s1m, r1m, z1s, z1r, z.nc)
    vals = r1m[...]
    lane1 = lanes_of((z.r1, z.rl))
    member = (vals.astype(F32) > 0.0) & (lane1 < z.experts)
    rank = mm(before(z.r1), member.astype(F32).astype(BF))
    rank = jnp.where(member, rank, -1.0).astype(BF)
    er, el = lanes_of((z.rl, z.pairs), 0) - g * z.gs, lanes_of((z.rl, z.pairs), 1)
    expand = ((el >= er * z.sl) & (el < (er + 1) * z.sl)).astype(F32).astype(BF)
    place = (lanes_of((z.r1, z.pairs)) & (z.sl - 1)).astype(F32)
    t_mat[...] = (mm(rank, expand) == place).astype(F32).astype(BF)

    def pack_two(c):
        group_wait(s1.at[c], r1.at[c], z1s, z1r, c)
        s2[c] = mm(t_mat[...], r1[c], 0, 0).astype(BF)
        plane_send(s2.at[c], x2.at[c], p2s, p2r, c)
        pair_send(x2.at[c, prows(p)], y2.at[c, prows(p)], fs.at[c, 0], fr.at[c, 0])

    def accumulate(x, half, c):
        if c < z.half_chunks:
            at = cols_at(half, c)
            gate_add, up_add = mm(x, gate_ref[at, :]), mm(x, up_ref[at, :])
            gacc[...] += gate_add
            uacc[...] += up_add
        else:
            pacc[...] += mm(x, down_ref[:, cols_at(half, c - z.half_chunks)], 1, 1)

    def land(c):
        for d in range(1, z.gs):
            plane_wait_one(s2.at[c], x2.at[c], p2s, p2r, c, d)
            q = (p + z.gs - d) % z.gs
            pair_send(x2.at[c, prows(q)], y2.at[c, prows(q)], fs.at[c, d], fr.at[c, d])
        accumulate(x2[c], t, c)

    def land_other(c):
        for d in range(z.gs):
            q = (p + z.gs - d) % z.gs
            rcopy(x2.at[c, prows(q)], y2.at[c, prows(q)], fs.at[c, d], fr.at[c, d], e, other).wait_recv()
        accumulate(y2[c], other, c)

    gacc[...] = jnp.zeros_like(gacc)
    uacc[...] = jnp.zeros_like(uacc)
    pacc[...] = jnp.zeros_like(pacc)
    for c in range(z.nc + 3):
        if c < z.nc:
            pack_two(c)
        if c == z.nc - 1:
            group_wait(s1w, r1w, z1s, z1r, z.nc + 1)
            s2m[...] = mm(t_mat[...], r1w[...], 0, 0).astype(BF)
            plane_send(s2m, x2m, p2s, p2r, z.nc)
        if 2 <= c < z.nc + 2:
            land(c - 2)
        if c >= 3:
            land_other(c - 3)
    plane_wait(s2m, x2m, p2s, p2r, z.nc)

    lane2 = lanes_of((z.pairs, z.rl))
    scale = jnp.sum(jnp.where(lane2 == e, x2m[...].astype(F32), 0.0), axis=1, keepdims=True)
    wcol[...] = jnp.broadcast_to(scale, wcol.shape)
    gate_pre, up_pre, pulled = gacc[...], uacc[...], pacc[...]
    sig = 1.0 / (1.0 + jnp.exp(-gate_pre))
    silu = gate_pre * sig
    hidden = (silu * up_pre).astype(BF)
    hid[...] = hidden
    wp[...] = jnp.broadcast_to(
        jnp.sum(pulled * hidden.astype(F32), axis=1, keepdims=True), wp.shape
    )
    w_copy = pair_send(wp, wpr, ms.at[0], mr.at[0])
    dh = scale * pulled
    dcat[:, : z.ff] = (dh * up_pre * sig * (1.0 + gate_pre * (1.0 - sig))).astype(BF)
    dcat[:, z.ff :] = (dh * silu).astype(BF)

    def token_term(half, k):
        at = cols_at(half, k)
        return (
            mm(dcat[:, : z.ff], gate_ref[at, :], 1, 1) + mm(dcat[:, z.ff :], up_ref[at, :], 1, 1)
        ).astype(BF)

    pt = []
    for k in range(z.half_chunks):
        pts[k] = token_term(other, k)
        pt.append(pair_send(pts.at[k], ptr.at[k], ptsm.at[k], ptrm.at[k]))
    w_copy.wait_recv()
    wsum = wp[:, 0:1] + wpr[:, 0:1]
    s3m[...] = jnp.where(lane2 == e, wsum, 0.0).astype(BF)
    plane_send(s3m, r3m, r3s, r3r, z.half_chunks)
    for k in range(z.half_chunks):
        pto[k] = token_term(t, k)
        pt[k].wait_recv()
        s3[k] = (pto[k].astype(F32) + ptr[k].astype(F32)).astype(BF)
        plane_send(s3.at[k], r3.at[k], r3s, r3r, k)

    ones_ff = jnp.ones((16, z.ff), BF)

    def gate_up_grads(xs, half, k):
        at = cols_at(half, k)
        total = mm(xs[k], dcat[...], 0, 0)
        gate_out[at, :] = total[:, : z.ff].astype(BF)
        up_out[at, :] = total[:, z.ff :].astype(BF)
        square = (total * total).astype(BF)
        sq[0:1, at] = mm(ones_ff, square[:, : z.ff], 1, 1)[0:1]
        sq[1:2, at] = mm(ones_ff, square[:, z.ff :], 1, 1)[0:1]

    def down_grads(xs, half, k):
        scaled = (wcol[:, 0:1] * xs[z.half_chunks + k].astype(F32)).astype(BF)
        total = mm(hid[...], scaled, 0, 0)
        down_out[:, cols_at(half, k)] = total.astype(BF)
        return mm(jnp.ones((16, z.cc), BF), (total * total).astype(BF), 1, 1)[0:1]

    def back_two(k):
        plane_wait(s3.at[k], r3.at[k], r3s, r3r, k)
        s4[k] = mm(t_mat[...], r3[k]).astype(BF)
        group_send(s4.at[k], r4.at[k], r4s, r4r, k)

    gate_up_grads(x2, t, 0)
    plane_wait(s3m, r3m, r3s, r3r, z.half_chunks)
    s4m[...] = mm(t_mat[...], r3m[...]).astype(BF)
    group_send(s4m, r4m, r4s, r4r, z.half_chunks)
    gate_up_grads(x2, t, 1)
    for k in range(z.half_chunks - 1):
        back_two(k)
        if k + 2 < z.half_chunks:
            gate_up_grads(x2, t, k + 2)
        else:
            gate_up_grads(y2, other, 0)

    group_wait(s4m, r4m, r4s, r4r, z.half_chunks)
    dw = mm(s_mat[...], r4m[...])
    dpicked = jnp.sum(dw * paired, axis=1, keepdims=True)
    q = picked * dw
    dchosen = paired * (q - jnp.sum(paired * q, axis=1, keepdims=True))
    dgroup = jnp.where(is_group, (dpicked * picked) * (ghot - gprob), 0.0)
    dall = (dchosen + dgroup).astype(BF)
    dterm = dall[:, : z.rw] if z.rw < z.rl else dall
    tcopies = []
    if z.reduce_here:
        full = mm(dterm, tok_ref[...], 0, 0)
        for i in range(z.n_ep):
            term[i] = full[:, i * z.ch : (i + 1) * z.ch]

        def term_copy(m):
            to = (e + 2 * m + t) % z.n_ep
            return rcopy(term.at[to], trec.at[m], ts.at[m], tr.at[m], to, t)

        @pl.when(t == 0)
        def _():
            trec[0] = term[e]

        @pl.when(t == 1)
        def _():
            term_copy(0).start()

        for m in range(1, z.n_ep // 2):
            term_copy(m).start()
    else:
        row = lanes_of((z.rows, z.rl), 0)[:, : dterm.shape[1]]
        mine = (row >= t * (z.rows // 2)) & (row < (t + 1) * (z.rows // 2))
        dterm = jnp.where(mine, dterm.astype(F32), 0.0).astype(BF)
        rout_out[...] = mm(dterm, tok_ref[...], 0, 0)

    back_two(z.half_chunks - 1)
    for k in range(1, z.half_chunks):
        gate_up_grads(y2, other, k)
    sq_copy = pair_send(sq, sqr, ms.at[1], mr.at[1])
    dsq = jnp.zeros((1, z.ff), F32)
    for k in range(z.half_chunks):
        dsq += down_grads(x2, t, k)

    if z.reduce_here:

        @pl.when(t == 1)
        def _():
            term_copy(0).wait_recv()

        for m in range(1, z.n_ep // 2):
            term_copy(m).wait_recv()
        acc = trec[0]
        for m in range(1, z.n_ep // 2):
            acc = acc + trec[m]
        tsum[...] = acc
        t_pair = pair_send(tsum, tsumr, ms.at[2], mr.at[2])
    for k in range(z.half_chunks):
        dsq += down_grads(y2, other, k)
    dsq_out[...] = dsq

    for k in range(z.half_chunks):
        group_wait(s4.at[k], r4.at[k], r4s, r4r, k)
        tg_out[:, k * z.cc : (k + 1) * z.cc] = (
            mm(s_mat[...], r4[k]) + mm(dall, rc_ref[:, cols_at(t, k)])
        ).astype(BF)
    sq_copy.wait_recv()
    gsq_out[...] = sq[0:1, :] + sqr[0:1, :]
    usq_out[...] = sq[1:2, :] + sqr[1:2, :]
    if z.reduce_here:
        t_pair.wait_recv()
        rout_out[...] = tsum[...] + tsumr[...]

        @pl.when(t == 1)
        def _():
            term_copy(0).wait_send()

        for m in range(1, z.n_ep // 2):
            term_copy(m).wait_send()
    for cp in sends:
        cp.wait_send()


def finish(
    z, gate_in, up_in, down_in, tg_in, gsq_in, usq_in, dsq_in, rout_in,
    gate_out, up_out, down_out, tg_out, gsq_out, usq_out, dsq_out, reg_out, rgg_out, rows_out, sem,
):
    copies = []
    pairs = (
        (gate_in, gate_out), (up_in, up_out), (down_in, down_out), (tg_in, tg_out),
        (gsq_in, gsq_out), (usq_in, usq_out), (dsq_in, dsq_out),
    )
    for i, (src, dst) in enumerate(pairs):
        cp = pltpu.make_async_copy(src, dst, sem.at[i])
        cp.start()
        copies.append(cp)
    half = z.ch // 2
    both = rout_in[...]
    mine = jnp.where(lax.axis_index("tp") == 0, both[:, :half], both[:, half:])
    reg = mine[: z.experts]
    rgg = mine[z.experts : z.experts + z.groups]
    reg_out[...] = reg
    rgg_out[...] = rgg
    rows_out[...] = jnp.sum(reg * reg, axis=0, keepdims=True) + jnp.sum(rgg * rgg, axis=0, keepdims=True)
    for cp in copies:
        cp.wait()


def body(axes, tokens, cotangent, routes, router_group, router_expert, gate_proj, up_proj, down_proj):
    z = sizes_of(axes, tokens, routes, router_group, router_expert, gate_proj)
    h, nc, cc = z.half_chunks, z.nc, z.cc
    rout_shape = (z.rw, z.ch) if z.reduce_here else (min(z.rw, z.rl), z.width)
    outs = [
        ((z.rows, z.cw), BF), ((z.width, z.ff), BF), ((z.width, z.ff), BF), ((z.ff, z.width), BF),
        ((1, z.width), F32), ((1, z.width), F32), ((1, z.ff), F32), (rout_shape, F32),
    ]
    V = pltpu.VMEM
    chd = z.ch if z.reduce_here else 128
    scratch = [
        V((z.rl, z.width), BF), V((z.r1, z.rl), BF), V((z.r1, z.rl), BF),
        V((z.rows, z.r1), BF), V((z.r1, z.pairs), BF),
        V((z.r1, z.rl), BF), V((z.r1, z.rl), BF),
        V((nc, z.r1, cc), BF), V((nc, z.r1, cc), BF),
        V((z.pairs, z.rl), BF), V((z.pairs, z.rl), BF),
        V((nc, z.pairs, cc), BF), V((nc, z.pairs, cc), BF),
        V((8, 128), BF), V((nc, z.pairs, cc), BF),
        V((z.pairs, z.ff), F32), V((z.pairs, z.ff), F32), V((z.pairs, z.ff), F32),
        V((z.pairs, 2 * z.ff), BF), V((z.pairs, z.ff), BF), V((z.pairs, 128), F32),
        V((z.pairs, 128), F32), V((z.pairs, 128), F32),
        V((h, z.pairs, cc), BF), V((h, z.pairs, cc), BF), V((h, z.pairs, cc), BF),
        V((z.pairs, z.rl), BF), V((z.pairs, z.rl), BF),
        V((h, z.pairs, cc), BF), V((h, z.pairs, cc), BF),
        V((z.r1, z.rl), BF), V((z.r1, z.rl), BF),
        V((h, z.r1, cc), BF), V((h, z.r1, cc), BF),
        V((2, z.width), F32), V((2, z.width), F32),
        V((z.n_ep, z.rw, chd), F32), V((z.n_ep // 2, z.rw, chd), F32),
        V((z.rw, chd), F32), V((z.rw, chd), F32),
    ]
    D = pltpu.SemaphoreType.DMA
    sems = [
        D((nc + 2, z.groups)), D((nc + 2, z.groups)), D((nc + 1, z.gs)), D((nc + 1, z.gs)),
        D((nc, z.gs)), D((nc, z.gs)), D((h,)), D((h,)),
        D((h + 1, z.gs)), D((h + 1, z.gs)), D((h + 1, z.groups)), D((h + 1, z.groups)),
        D((3,)), D((3,)), D((z.n_ep // 2,)), D((z.n_ep // 2,)),
    ]
    spec = pl.BlockSpec(memory_space=pltpu.VMEM)
    tg, gate, up, down, gsq, usq, dsq, rout = pl.pallas_call(
        functools.partial(kernel, z),
        out_shape=[jax.ShapeDtypeStruct(s, d) for s, d in outs],
        in_specs=[spec] * 8,
        out_specs=[spec] * len(outs),
        scratch_shapes=scratch + sems,
        compiler_params=pltpu.CompilerParams(
            collective_id=0, has_side_effects=True, vmem_limit_bytes=44 * 2**20
        ),
    )(tokens, cotangent, routes.T, router_expert.T, router_group.T, gate_proj[0], up_proj[0], down_proj[0])
    if z.reduce_here:
        half = z.ch // 2
        shapes = [gate, up, down, tg, gsq, usq, dsq]
        anywhere = pl.BlockSpec(memory_space=pl.ANY)
        gate, up, down, tg, gsq, usq, dsq, reg, rgg, rrows = pl.pallas_call(
            functools.partial(finish, z),
            out_shape=[jax.ShapeDtypeStruct(a.shape, a.dtype) for a in shapes]
            + [jax.ShapeDtypeStruct((n, half), F32) for n in (z.experts, z.groups, 1)],
            in_specs=[spec] * 8,
            out_specs=[anywhere] * 7 + [spec] * 3,
            scratch_shapes=[D((7,))],
            compiler_params=pltpu.CompilerParams(vmem_limit_bytes=16 * 2**20),
        )(*shapes, rout)
        reg, rgg, rrows = reg.T, rgg.T, rrows[0]
    else:
        mine = lax.psum_scatter(rout.T, ("ep", "tp"), scatter_dimension=0, tiled=True)
        reg = mine[:, : z.experts]
        rgg = mine[:, z.experts : z.experts + z.groups]
        rrows = jnp.sum(reg * reg, axis=1) + jnp.sum(rgg * rgg, axis=1)
    return (tg, gate[None], up[None], down[None], gsq, usq, dsq, reg, rgg, rrows)


def solution(mesh):
    return jax.shard_map(
        functools.partial(body, dict(mesh.shape)),
        mesh=mesh,
        in_specs=(
            P("ep", None), P("ep", None), P("ep", None), P(), P(),
            P("ep", None, "tp"), P("ep", None, "tp"), P("ep", "tp", None),
        ),
        out_specs=(
            P("ep", "tp"), P("ep", None, "tp"), P("ep", None, "tp"), P("ep", "tp", None),
            P("ep", None), P("ep", None), P("ep", "tp"),
            P(("ep", "tp"), None), P(("ep", "tp"), None), P(("ep", "tp")),
        ),
        check_vma=False,
    )
```

profile of v0, /device:TPU:0, one launch (start us, length us, event | category | flops | bytes accessed | tf_op | source)
XLA Modules:
  0.0 82.0 jit_solution(9604853336849357922)
XLA Ops:
  0.6 0.0 copy-start.7
  0.7 0.7 copy-done.7
  1.3 0.0 copy-start
  1.3 1.2 %copy-done = bf16[1,2048,256]{2,1,0:T(8,128)(2,1)S(1)} copy-done((bf16[1,2048,256]{2,1,0:T(8,128)(2,1)S(1)}, bf16[1,2048,256]{2,1,0:T(8,128)(2,1)}, u32[]{:S(2)}) %copy-start) | copy-done | bytes 1048600
  2.6 0.0 copy-start.1
  2.6 1.2 %copy-done.1 = bf16[1,2048,256]{2,1,0:T(8,128)(2,1)S(1)} copy-done((bf16[1,2048,256]{2,1,0:T(8,128)(2,1)S(1)}, bf16[1,2048,256]{2,1,0:T(8,128)(2,1)}, u32[]{:S(2)}) %copy-start.1) | copy-done | bytes 1048600
  3.8 0.0 copy-start.2
  3.8 1.2 %copy-done.2 = bf16[1,256,2048]{2,1,0:T(8,128)(2,1)S(1)} copy-done((bf16[1,256,2048]{2,1,0:T(8,128)(2,1)S(1)}, bf16[1,256,2048]{2,1,0:T(8,128)(2,1)}, u32[]{:S(2)}) %copy-start.2) | copy-done | bytes 1048600
  5.0 0.0 copy-start.3
  5.0 1.0 %copy-done.3 = bf16[128,2048]{1,0:T(8,128)(2,1)S(1)} copy-done((bf16[128,2048]{1,0:T(8,128)(2,1)S(1)}, bf16[128,2048]{1,0:T(8,128)(2,1)}, u32[]{:S(2)}) %copy-start.3) | copy-done | bytes 524312
  6.0 0.0 copy-start.4
  6.0 1.0 %copy-done.4 = bf16[128,2048]{1,0:T(8,128)(2,1)S(1)} copy-done((bf16[128,2048]{1,0:T(8,128)(2,1)S(1)}, bf16[128,2048]{1,0:T(8,128)(2,1)}, u32[]{:S(2)}) %copy-start.4) | copy-done | bytes 524312
  7.1 0.0 copy-start.5
  7.1 0.8 %copy-done.5 = bf16[2048,16]{0,1:T(8,128)(2,1)S(1)} copy-done((bf16[2048,16]{0,1:T(8,128)(2,1)S(1)}, bf16[2048,16]{0,1:T(8,128)(2,1)}, u32[]{:S(2)}) %copy-start.5) | copy-done | bytes 65560
  7.9 0.0 copy-start.6
  7.9 0.7 copy-done.6
  8.6 70.8 %shard_map.159 = (bf16[128,1024]{1,0:T(8,128)(2,1)S(1)}, bf16[2048,256]{1,0:T(8,128)(2,1)S(1)}, bf16[2048,256]{1,0:T(8,128)(2,1)S(1)}, bf16[256,2048]{1,0:T(8,12...) custom-call(bf16[128,2048]{1,0:T(8,128)(2,1)S(1)} %copy-done.3, ...), custom_call_target="tpu_custom_call" | custom-call | tf_op jit(solution)/shard_map/pallas_call | solution.py:438
  79.4 2.4 %shard_map.160 = (bf16[2048,256]{1,0:T(8,128)(2,1)}, bf16[2048,256]{1,0:T(8,128)(2,1)}, bf16[256,2048]{1,0:T(8,128)(2,1)}, bf16[128,1024]{1,0:T(8,128)(2,1)}, f3...) custom-call(bf16[2048,256]{1,0:T(8,128)(2,1)S(1)} %get-tuple-element, ...), custom_call_target="tpu_custom_call" | custom-call | tf_op jit(solution)/shard_map/pallas_call | solution.py:452
Async XLA Ops:
  0.6 0.7 copy-start.7
  1.3 1.2 %copy-start = (bf16[1,2048,256]{2,1,0:T(8,128)(2,1)S(1)}, bf16[1,2048,256]{2,1,0:T(8,128)(2,1)}, u32[]{:S(2)}) copy-start(bf16[1,2048,256]{2,1,0:T(8,128)(2,1)} %param.13) | copy-start | bytes 3145732
  2.6 1.2 %copy-start.1 = (bf16[1,2048,256]{2,1,0:T(8,128)(2,1)S(1)}, bf16[1,2048,256]{2,1,0:T(8,128)(2,1)}, u32[]{:S(2)}) copy-start(bf16[1,2048,256]{2,1,0:T(8,128)(2,1)} %param.14) | copy-start | bytes 3145732
  3.8 1.2 %copy-start.2 = (bf16[1,256,2048]{2,1,0:T(8,128)(2,1)S(1)}, bf16[1,256,2048]{2,1,0:T(8,128)(2,1)}, u32[]{:S(2)}) copy-start(bf16[1,256,2048]{2,1,0:T(8,128)(2,1)} %param.15) | copy-start | bytes 3145732
  5.0 1.0 %copy-start.3 = (bf16[128,2048]{1,0:T(8,128)(2,1)S(1)}, bf16[128,2048]{1,0:T(8,128)(2,1)}, u32[]{:S(2)}) copy-start(bf16[128,2048]{1,0:T(8,128)(2,1)} %tok_ref.1) | copy-start | bytes 1572868
  6.0 1.0 %copy-start.4 = (bf16[128,2048]{1,0:T(8,128)(2,1)S(1)}, bf16[128,2048]{1,0:T(8,128)(2,1)}, u32[]{:S(2)}) copy-start(bf16[128,2048]{1,0:T(8,128)(2,1)} %cot_ref.1) | copy-start | bytes 1572868
  7.1 0.8 %copy-start.5 = (bf16[2048,16]{0,1:T(8,128)(2,1)S(1)}, bf16[2048,16]{0,1:T(8,128)(2,1)}, u32[]{:S(2)}) copy-start(bf16[2048,16]{0,1:T(8,128)(2,1)} %param.12) | copy-start | bytes 196612
  7.9 0.7 copy-start.6
where the time goes:
time: 82.5 us; the launch traced here: 82 us
  Pallas kernels  73.2 us (89%)
  local copies, waits for them, and re-layouts  7.98 us (10%)
  between operations  0.83 us (1%)
    pallas_call x1, Pallas kernels, body(): pl.pallas_call(functools.partial(kernel, z), out_shape=[jax.ShapeDtypeStr...  70.8 us
    unnamed x16, local copies, waits for them, and re-layouts  7.98 us
    pallas_call x1, Pallas kernels, body(): pl.pallas_call(functools.partial(finish, z), out_shape=[jax.ShapeDtypeStr...  2.42 us

commit v1 on v0

--- a/solution.py
+++ b/solution.py
@@ -372,6 +372,452 @@
         cp.wait_send()
 
 
+def sourced(
+    z, tok_h, cot_h, routes_h, rexp_h, rgrp_h, gate_h, up_h, down_h,
+    tg_out, gate_out, up_out, down_out, gsq_out, usq_out, dsq_out, rout_out,
+    tok_ref, cot_ref, routes_ref, rexp_ref, rgrp_ref, gate_ref, up_ref, down_ref,
+    rc_ref, s_mat, s_tr, t_mat, t_tr, s1m, r1m, s1w, r1w, s1, r1, s2m, x2m, s2, x2, y2,
+    gacc, uacc, dcat, hid, wcol, wp, wpr, pts, ptr, s3m, r3m, s3, r3, s4, r4, dall_ref,
+    sq, sqr, term, tra, tsa, trb, tsum, tsumr,
+    ins, z1s, z1r, p2s, p2r, fs, fr, ws, wr, ptsm, ptrm, r3s, r3r, r4s, r4r, ms, mr, tas, tar, tbs, tbr,
+):
+    e, t = lax.axis_index("ep"), lax.axis_index("tp")
+    g, p = e // z.gs, e % z.gs
+    other = 1 - t
+    hk = [g, g + 1 - 2 * (g % 2), 3 - g, (g + 2) % 4]
+    qd = [p, p + 1 - 2 * (p % 2), (p + 2) % 4, 3 - p]
+    nj, cc, gr, cap, blk, per = z.nj, z.cc, z.gr, z.cap, z.blk, z.per
+    ng = 2 * nj
+    far = (1, 2, 3)
+
+    def rcopy(src, dst, ss, rs, ep, tp):
+        return pltpu.make_async_remote_copy(
+            src_ref=src, dst_ref=dst, send_sem=ss, recv_sem=rs,
+            device_id=(ep, tp), device_id_type=MESH,
+        )
+
+    barrier = pltpu.get_barrier_semaphore()
+    for k in far:
+        pl.semaphore_signal(barrier, inc=1, device_id=(hk[k] * z.gs + p, t), device_id_type=MESH)
+        pl.semaphore_signal(barrier, inc=1, device_id=(g * z.gs + qd[k], t), device_id_type=MESH)
+    pl.semaphore_signal(barrier, inc=1, device_id=(e, other), device_id_type=MESH)
+
+    loads = [
+        pltpu.make_async_copy(a, b, ins.at[i])
+        for i, (a, b) in enumerate((
+            (routes_h, routes_ref), (tok_h, tok_ref), (rexp_h, rexp_ref), (rgrp_h, rgrp_ref),
+            (cot_h, cot_ref), (gate_h, gate_ref), (up_h, up_ref), (down_h, down_ref),
+        ))
+    ]
+    for cp in loads:
+        cp.start()
+
+    sends = []
+
+    def go(cp):
+        cp.start()
+        sends.append(cp)
+        return cp
+
+    def kr(k):
+        return pl.ds(k * gr, gr)
+
+    def kb(k):
+        return pl.ds(k * blk, blk)
+
+    def slot(q):
+        return pl.ds(pl.multiple_of(q * cap, cap), cap)
+
+    def in_block(k, q):
+        return pl.ds(pl.multiple_of(k * blk + q * cap, cap), cap)
+
+    def cols(half, j):
+        return pl.ds(pl.multiple_of(half * z.cw + j * cc, cc), cc)
+
+    def z_send(src, dst, c, k):
+        go(rcopy(src.at[kr(k)], dst.at[kr(k)], z1s.at[c, k], z1r.at[c, k], hk[k] * z.gs + p, t))
+
+    def z_wait(src, dst, c, k):
+        rcopy(src.at[kr(k)], dst.at[kr(k)], z1s.at[c, k], z1r.at[c, k], hk[k] * z.gs + p, t).wait_recv()
+
+    def plane_send(src, dst, c, k):
+        for d in (3, 1, 2):
+            go(rcopy(src.at[in_block(k, qd[d])], dst.at[in_block(k, p)], p2s.at[c, k, d], p2r.at[c, k, d],
+                     g * z.gs + qd[d], t))
+        dst[in_block(k, p), :] = src[in_block(k, p), :]
+
+    def plane_wait(src, dst, c, k):
+        for d in (1, 2, 3):
+            rcopy(src.at[in_block(k, qd[d])], dst.at[in_block(k, qd[d])], p2s.at[c, k, d], p2r.at[c, k, d],
+                  g * z.gs + qd[d], t).wait_recv()
+
+    def back_send(src, dst, c, k):
+        for d in (3, 1, 2):
+            go(rcopy(src.at[in_block(k, qd[d])], dst.at[in_block(k, p)], r3s.at[c, k, d], r3r.at[c, k, d],
+                     g * z.gs + qd[d], t))
+        dst[in_block(k, p), :] = src[in_block(k, p), :]
+
+    def back_wait(src, dst, c, k):
+        for d in (1, 2, 3):
+            rcopy(src.at[in_block(k, qd[d])], dst.at[in_block(k, qd[d])], r3s.at[c, k, d], r3r.at[c, k, d],
+                  g * z.gs + qd[d], t).wait_recv()
+
+    def pair(src, dst, ss, rs):
+        return rcopy(src, dst, ss, rs, e, other)
+
+    lane = lanes_of((z.rows, z.rl))
+    ll, lb = lane % per, lane // per
+    eye = lanes_of((z.rows, z.rows), 0) == lanes_of((z.rows, z.rows), 1)
+
+    def column(row):
+        return jnp.sum(jnp.where(eye, row.astype(F32), 0.0), axis=1, keepdims=True).astype(jnp.int32)
+
+    def before(n):
+        return (lanes_of((n, n), 1) < lanes_of((n, n), 0)).astype(F32).astype(BF)
+
+    loads[0].wait()
+    r0, r1_ = column(routes_ref[0:1, :]), column(routes_ref[1:2, :])
+    chosen = (ll == r0) | (ll == r1_)
+    low = (ll - z.experts) * z.gs
+    is_group = (ll >= z.experts) & (ll < z.experts + z.groups)
+    in_group = is_group & (r0 >= low) & (r0 < low + z.gs)
+    grank = mm(before(z.rows), in_group.astype(F32).astype(BF))
+    grank = jnp.where(in_group, grank, -1.0).astype(BF)
+    er, el = lanes_of((z.rl, z.r1), 0) - z.experts, lanes_of((z.rl, z.r1), 1)
+    kk = el // gr
+    want = jnp.where(kk == 0, hk[0], jnp.where(kk == 1, hk[1], jnp.where(kk == 2, hk[2], hk[3])))
+    expand = (er == want).astype(F32).astype(BF)
+    place = (lanes_of((z.rows, z.r1)) % gr).astype(F32)
+    s_f = (mm(grank, expand) == place).astype(F32)
+    s_mat[...] = s_f.astype(BF)
+    s_tr[...] = s_f.T.astype(BF)
+    s1m[...] = mm(s_tr[...], jnp.where(chosen & (lb == 0), 1.0, 0.0).astype(BF)).astype(BF)
+    r1m[kr(0), :] = s1m[kr(0), :]
+
+    def fill(c):
+        j = c % nj
+        src = tok_ref if c < nj else cot_ref
+        s1[c] = mm(s_tr[...], src[:, cols(t, j)]).astype(BF)
+        r1[c, kr(0), :] = s1[c, kr(0), :]
+
+    loads[1].wait()
+    fill(0)
+    pl.semaphore_wait(barrier, 7)
+    for k in far:
+        z_send(s1m, r1m, ng, k)
+    for k in (1, 2):
+        z_send(s1.at[0], r1.at[0], 0, k)
+    for c in range(1, nj):
+        fill(c)
+        for k in (1, 2):
+            z_send(s1.at[c], r1.at[c], c, k)
+
+    def make_t(k):
+        if k:
+            z_wait(s1m, r1m, ng, k)
+        vals = r1m[kr(k), :]
+        ln = lanes_of((gr, z.rl))
+        member = (vals.astype(F32) > 0.0) & (ln < z.experts)
+        rank = mm(before(gr), member.astype(F32).astype(BF))
+        rank = jnp.where(member, rank, -1.0).astype(BF)
+        sr, sc = lanes_of((z.rl, blk), 0) - g * z.gs, lanes_of((z.rl, blk), 1)
+        spread = (sr == sc // cap).astype(F32).astype(BF)
+        spot = (lanes_of((gr, blk)) % cap).astype(F32)
+        tf = (mm(rank, spread) == spot).astype(F32)
+        t_mat[k] = tf.astype(BF)
+        t_tr[k] = tf.T.astype(BF)
+
+    def op_a(k, c):
+        if k:
+            z_wait(s1.at[c], r1.at[c], c, k)
+        s2[c, kb(k), :] = mm(t_tr[k], r1[c, kr(k), :]).astype(BF)
+        plane_send(s2.at[c], x2.at[c], c, k)
+
+    def op_am(k):
+        if k:
+            z_wait(s1w, r1w, ng + 1, k)
+        s2m[kb(k), :] = mm(t_tr[k], r1w[kr(k), :]).astype(BF)
+        plane_send(s2m, x2m, ng, k)
+
+    make_t(0)
+    for c in range(nj):
+        op_a(0, c)
+
+    rc_ref[...] = jnp.zeros_like(rc_ref)
+    loads[2].wait()
+    loads[3].wait()
+    for b in range(z.rl // per):
+        rc_ref[b * per : b * per + z.experts, :] = rexp_ref[...]
+        rc_ref[b * per + z.experts : b * per + z.experts + z.groups, :] = rgrp_ref[...]
+    expd = jnp.exp(mm(tok_ref[...], rc_ref[...], 1, 1))
+    gexp = jnp.where(is_group, expd, 0.0)
+    gprob = gexp / jnp.sum(jnp.where(lb == 0, gexp, 0.0), axis=1, keepdims=True)
+    picked = jnp.sum(jnp.where(in_group & (lb == 0), gprob, 0.0), axis=1, keepdims=True)
+    pexp = jnp.where(chosen, expd, 0.0)
+    paired = pexp / jnp.sum(jnp.where(lb == 0, pexp, 0.0), axis=1, keepdims=True)
+    both = paired + gprob
+    upper = both.astype(BF).astype(F32)
+    meta = jnp.where(lb == 1, picked * paired, jnp.where(lb == 2, upper, jnp.where(lb == 3, both - upper, 0.0)))
+    s1w[...] = mm(s_tr[...], meta.astype(BF)).astype(BF)
+    r1w[kr(0), :] = s1w[kr(0), :]
+    for k in far:
+        z_send(s1w, r1w, ng + 1, k)
+    loads[4].wait()
+    for c in range(nj, ng):
+        fill(c)
+        for k in (1, 2):
+            z_send(s1.at[c], r1.at[c], c, k)
+        op_a(0, c)
+    for c in range(ng):
+        z_send(s1.at[c], r1.at[c], c, 3)
+    op_am(0)
+
+    def op_b(k, c):
+        plane_wait(s2.at[c], x2.at[c], c, k)
+        go(pair(x2.at[c, kb(k)], y2.at[c, kb(k)], fs.at[c, k], fr.at[c, k]))
+
+    def y_wait(k, c):
+        pair(x2.at[c, kb(k)], y2.at[c, kb(k)], fs.at[c, k], fr.at[c, k]).wait_recv()
+
+    def op_c1(k):
+        ga = ua = None
+        for half, xs in ((t, x2), (other, y2)):
+            for j in range(nj):
+                if xs is y2:
+                    y_wait(k, j)
+                x, at = xs[j, kb(k), :], cols(half, j)
+                a, b = mm(x, gate_ref[at, :]), mm(x, up_ref[at, :])
+                ga, ua = (a, b) if ga is None else (ga + a, ua + b)
+        gacc[...] = ga
+        uacc[...] = ua
+
+    lane2 = lanes_of((blk, z.rl))
+
+    def token_term(k, half, j):
+        at = cols(half, j)
+        return (
+            mm(dcat[kb(k), : z.ff], gate_ref[at, :], 1, 1) + mm(dcat[kb(k), z.ff :], up_ref[at, :], 1, 1)
+        ).astype(BF)
+
+    def op_c2(k):
+        pulled = None
+        for half, xs in ((t, x2), (other, y2)):
+            for j in range(nj):
+                if xs is y2:
+                    y_wait(k, nj + j)
+                a = mm(xs[nj + j, kb(k), :], down_ref[:, cols(half, j)], 1, 1)
+                pulled = a if pulled is None else pulled + a
+        plane_wait(s2m, x2m, ng, k)
+        scale = jnp.sum(jnp.where(lane2 == per + e, x2m[kb(k), :].astype(F32), 0.0), axis=1, keepdims=True)
+        wcol[kb(k), :] = jnp.broadcast_to(scale, (blk, z.rl))
+        gate_pre, up_pre = gacc[...], uacc[...]
+        sig = 1.0 / (1.0 + jnp.exp(-gate_pre))
+        silu = gate_pre * sig
+        hidden = (silu * up_pre).astype(BF)
+        hid[kb(k), :] = hidden
+        wp[kb(k), :] = jnp.broadcast_to(
+            jnp.sum(pulled * hidden.astype(F32), axis=1, keepdims=True), (blk, z.rl)
+        )
+        go(pair(wp.at[kb(k)], wpr.at[kb(k)], ws.at[k], wr.at[k]))
+        dh = scale * pulled
+        dcat[kb(k), : z.ff] = (dh * up_pre * sig * (1.0 + gate_pre * (1.0 - sig))).astype(BF)
+        dcat[kb(k), z.ff :] = (dh * silu).astype(BF)
+        for j in range(nj):
+            pts[j, kb(k), :] = token_term(k, other, j)
+            go(pair(pts.at[j, kb(k)], ptr.at[j, kb(k)], ptsm.at[j, k], ptrm.at[j, k]))
+
+    def op_d(k):
+        pair(wp.at[kb(k)], wpr.at[kb(k)], ws.at[k], wr.at[k]).wait_recv()
+        wsum = wp[kb(k), :] + wpr[kb(k), :]
+        s3m[kb(k), :] = jnp.where(lane2 == e, wsum, 0.0).astype(BF)
+        back_send(s3m, r3m, nj, k)
+        for j in range(nj):
+            mine = token_term(k, t, j)
+            pair(pts.at[j, kb(k)], ptr.at[j, kb(k)], ptsm.at[j, k], ptrm.at[j, k]).wait_recv()
+            s3[j, kb(k), :] = (mine.astype(F32) + ptr[j, kb(k), :].astype(F32)).astype(BF)
+            back_send(s3.at[j], r3.at[j], j, k)
+
+    def home_copy(j, k):
+        return rcopy(s4.at[j, kr(k)], r4.at[j, kr(k)], r4s.at[j, k], r4r.at[j, k], hk[k] * z.gs + p, t)
+
+    lane3 = lanes_of((gr, z.rl))
+    i1, i2 = lanes_of((z.rl, z.rl), 0), lanes_of((z.rl, z.rl), 1)
+    fold = ((i2 < per) & ((i1 == 2 * per + i2) | (i1 == 3 * per + i2))).astype(F32).astype(BF)
+
+    def op_f(k):
+        vals = mm(r1w[kr(k), :], fold)
+        pr = jnp.where(lane3 < z.experts, vals, 0.0)
+        gp = jnp.where((lane3 >= z.experts) & (lane3 < z.experts + z.groups), vals, 0.0)
+        here = lane3 == z.experts + g
+        pk = jnp.sum(jnp.where(here, vals, 0.0), axis=1, keepdims=True)
+        back_wait(s3m, r3m, nj, k)
+        dw = mm(t_mat[k], r3m[kb(k), :])
+        dpicked = jnp.sum(dw * pr, axis=1, keepdims=True)
+        q = pk * dw
+        dchosen = pr * (q - jnp.sum(pr * q, axis=1, keepdims=True))
+        dgroup = (dpicked * pk) * (here.astype(F32) - gp)
+        dgroup = jnp.where((lane3 >= z.experts) & (lane3 < z.experts + z.groups), dgroup, 0.0)
+        dall = (dchosen + dgroup).astype(BF)
+        dall_ref[kr(k), :] = dall
+        for j in range(nj):
+            back_wait(s3.at[j], r3.at[j], j, k)
+            row = (mm(t_mat[k], r3[j, kb(k), :]) + mm(dall, rc_ref[:, cols(t, j)])).astype(BF)
+            if k:
+                s4[j, kr(k), :] = row
+                go(home_copy(j, k))
+            else:
+                r4[j, kr(k), :] = row
+
+    sub = min(cc, 256)
+    ns = cc // sub
+    ones_ff = jnp.ones((16, z.ff), BF)
+    ones_sub = jnp.ones((16, sub), BF)
+
+    def gate_up_grads(xs, half, i):
+        j, o = i // ns, (i % ns) * sub
+        at = pl.ds(pl.multiple_of(half * z.cw + i * sub, sub), sub)
+        total = mm(xs[j, :, o : o + sub], dcat[...], 0, 0)
+        gate_out[at, :] = total[:, : z.ff].astype(BF)
+        up_out[at, :] = total[:, z.ff :].astype(BF)
+        square = (total * total).astype(BF)
+        sq[0:1, at] = mm(ones_ff, square[:, : z.ff], 1, 1)[0:1]
+        sq[1:2, at] = mm(ones_ff, square[:, z.ff :], 1, 1)[0:1]
+
+    def down_grads(xs, half, i):
+        j, o = i // ns, (i % ns) * sub
+        at = pl.ds(pl.multiple_of(half * z.cw + i * sub, sub), sub)
+        scaled = (wcol[:, 0:1] * xs[nj + j, :, o : o + sub].astype(F32)).astype(BF)
+        total = mm(hid[...], scaled, 0, 0)
+        down_out[:, at] = total.astype(BF)
+        return mm(ones_sub, (total * total).astype(BF), 1, 1)[0:1]
+
+    for i in (5, 6, 7):
+        loads[i].wait()
+
+    def all_a(k, cs):
+        for c in cs:
+            op_a(k, c)
+
+    def all_b(k, cs):
+        for c in cs:
+            op_b(k, c)
+
+    tk, ct = range(nj), range(nj, ng)
+    make_t(1)
+    for c in range(ng):
+        op_a(1, c)
+        op_b(0, c)
+    op_am(1)
+    op_c1(0)
+    op_c2(0)
+    all_b(1, tk)
+    op_d(0)
+    all_b(1, ct)
+    make_t(2)
+    all_a(2, tk)
+    op_c1(1)
+    op_c2(1)
+    op_f(0)
+    all_a(2, ct)
+    op_am(2)
+    op_d(1)
+    all_b(2, tk)
+    make_t(3)
+    op_c1(2)
+    op_f(1)
+    all_b(2, ct)
+    op_c2(2)
+    op_d(2)
+    all_a(3, tk)
+    op_f(2)
+    all_a(3, ct)
+    op_am(3)
+    all_b(3, tk)
+    op_c1(3)
+    all_b(3, ct)
+    op_c2(3)
+    op_d(3)
+    n_piece = z.cw // sub
+    for i in range(n_piece):
+        gate_up_grads(x2, t, i)
+    op_f(3)
+
+    dterm = dall_ref[:, : z.rw]
+    half_chunks = z.cw // z.ch
+    for j in range(nj):
+        full = mm(dterm, r1[j], 0, 0)
+        for i in range(cc // z.ch):
+            n = j * (cc // z.ch) + i
+            term[n % z.gs, n // z.gs] = full[:, i * z.ch : (i + 1) * z.ch]
+
+    def term_a(d):
+        return rcopy(term.at[qd[d]], tra.at[d], tas.at[d], tar.at[d], g * z.gs + qd[d], t)
+
+    for d in far:
+        go(term_a(d))
+    per_core = half_chunks // z.gs
+
+    for i in range(n_piece):
+        gate_up_grads(y2, other, i)
+    sq_copy = go(pair(sq, sqr, ms.at[1], mr.at[1]))
+    for d in far:
+        term_a(d).wait_recv()
+    tsa[...] = term[p] + tra[1] + tra[2] + tra[3]
+    home_core = g // per_core
+
+    def term_b(k):
+        return rcopy(tsa.at[hk[k] % per_core], trb.at[k], tbs.at[k], tbr.at[k], hk[k] * z.gs + p, t)
+
+    for k in far:
+
+        @pl.when(hk[k] // per_core == t)
+        def _():
+            term_b(k).start()
+
+    dsq = jnp.zeros((1, z.ff), F32)
+    for i in range(n_piece):
+        dsq += down_grads(x2, t, i)
+    for i in range(n_piece):
+        dsq += down_grads(y2, other, i)
+    dsq_out[...] = dsq
+
+    t_pair = pair(tsum, tsumr, ms.at[2], mr.at[2])
+
+    @pl.when(home_core == t)
+    def _():
+        for k in far:
+            term_b(k).wait_recv()
+        tsum[...] = tsa[g % per_core] + trb[1] + trb[2] + trb[3]
+        t_pair.start()
+        rout_out[...] = tsum[...]
+
+    for j in range(nj):
+        for k in far:
+            home_copy(j, k).wait_recv()
+        tg_out[:, j * cc : (j + 1) * cc] = mm(s_mat[...], r4[j]).astype(BF)
+    sq_copy.wait_recv()
+    gsq_out[...] = sq[0:1, :] + sqr[0:1, :]
+    usq_out[...] = sq[1:2, :] + sqr[1:2, :]
+
+    @pl.when(home_core != t)
+    def _():
+        t_pair.wait_recv()
+        rout_out[...] = tsumr[...]
+
+    @pl.when(home_core == t)
+    def _():
+        t_pair.wait_send()
+
+    for k in far:
+
+        @pl.when(hk[k] // per_core == t)
+        def _():
+            term_b(k).wait_send()
+
+    for cp in sends:
+        cp.wait_send()
+
+
 def finish(
     z, gate_in, up_in, down_in, tg_in, gsq_in, usq_in, dsq_in, rout_in,
     gate_out, up_out, down_out, tg_out, gsq_out, usq_out, dsq_out, reg_out, rgg_out, rows_out, sem,
@@ -397,14 +843,62 @@
         cp.wait()
 
 
-def body(axes, tokens, cotangent, routes, router_group, router_expert, gate_proj, up_proj, down_proj):
-    z = sizes_of(axes, tokens, routes, router_group, router_expert, gate_proj)
+def by_source(z):
+    return (
+        z.reduce_here and z.groups == 4 and z.gs == 4 and z.cap % 16 == 0 and z.gr % 16 == 0
+        and z.experts + z.groups <= z.rl // 4 and z.cw % 512 == 0 and (z.cw // z.ch) % z.gs == 0
+    )
+
+
+def run_sourced(z, outs, tokens, cotangent, routes, router_group, router_expert, gate_proj, up_proj, down_proj):
+    z.nj = 2
+    z.cc = z.cw // z.nj
+    z.blk = z.gs * z.cap
+    z.per = z.rl // 4
+    nj, ng, cc = z.nj, 2 * z.nj, z.cc
+    V = pltpu.VMEM
+    args = (tokens, cotangent, routes.T, router_expert.T, router_group.T, gate_proj[0], up_proj[0], down_proj[0])
+    hb = z.cw // z.ch // z.gs
+    scratch = [V(a.shape, a.dtype) for a in args] + [
+        V((z.rl, z.width), BF), V((z.rows, z.r1), BF), V((z.r1, z.rows), BF),
+        V((z.groups, z.gr, z.blk), BF), V((z.groups, z.blk, z.gr), BF),
+        V((z.r1, z.rl), BF), V((z.r1, z.rl), BF), V((z.r1, z.rl), BF), V((z.r1, z.rl), BF),
+        V((ng, z.r1, cc), BF), V((ng, z.r1, cc), BF),
+        V((z.pairs, z.rl), BF), V((z.pairs, z.rl), BF),
+        V((ng, z.pairs, cc), BF), V((ng, z.pairs, cc), BF), V((ng, z.pairs, cc), BF),
+        V((z.blk, z.ff), F32), V((z.blk, z.ff), F32),
+        V((z.pairs, 2 * z.ff), BF), V((z.pairs, z.ff), BF), V((z.pairs, z.rl), F32),
+        V((z.pairs, z.rl), F32), V((z.pairs, z.rl), F32),
+        V((nj, z.pairs, cc), BF), V((nj, z.pairs, cc), BF),
+        V((z.pairs, z.rl), BF), V((z.pairs, z.rl), BF),
+        V((nj, z.pairs, cc), BF), V((nj, z.pairs, cc), BF),
+        V((nj, z.r1, cc), BF), V((nj, z.r1, cc), BF), V((z.r1, z.rl), BF),
+        V((2, z.width), F32), V((2, z.width), F32),
+        V((z.gs, hb, z.rw, z.ch), F32), V((z.gs, hb, z.rw, z.ch), F32), V((hb, z.rw, z.ch), F32),
+        V((z.groups, z.rw, z.ch), F32), V((z.rw, z.ch), F32), V((z.rw, z.ch), F32),
+    ]
+    D = pltpu.SemaphoreType.DMA
+    both = [
+        (ng + 2, 4), (ng + 1, 4, 4), (ng, 4), (4,), (nj, 4), (nj + 1, 4, 4), (nj, 4), (3,), (4,), (4,),
+    ]
+    sems = [D((len(args),))]
+    for s in both:
+        sems += [D(s), D(s)]
+    spec = pl.BlockSpec(memory_space=pltpu.VMEM)
+    return pl.pallas_call(
+        functools.partial(sourced, z),
+        out_shape=[jax.ShapeDtypeStruct(s, d) for s, d in outs],
+        in_specs=[pl.BlockSpec(memory_space=pltpu.HBM)] * len(args),
+        out_specs=[spec] * len(outs),
+        scratch_shapes=scratch + sems,
+        compiler_params=pltpu.CompilerParams(
+            collective_id=0, has_side_effects=True, vmem_limit_bytes=50 * 2**20
+        ),
+    )(*args)
+
+
+def run_wide(z, outs, tokens, cotangent, routes, router_group, router_expert, gate_proj, up_proj, down_proj):
     h, nc, cc = z.half_chunks, z.nc, z.cc
-    rout_shape = (z.rw, z.ch) if z.reduce_here else (min(z.rw, z.rl), z.width)
-    outs = [
-        ((z.rows, z.cw), BF), ((z.width, z.ff), BF), ((z.width, z.ff), BF), ((z.ff, z.width), BF),
-        ((1, z.width), F32), ((1, z.width), F32), ((1, z.ff), F32), (rout_shape, F32),
-    ]
     V = pltpu.VMEM
     chd = z.ch if z.reduce_here else 128
     scratch = [
@@ -435,7 +929,7 @@
         D((3,)), D((3,)), D((z.n_ep // 2,)), D((z.n_ep // 2,)),
     ]
     spec = pl.BlockSpec(memory_space=pltpu.VMEM)
-    tg, gate, up, down, gsq, usq, dsq, rout = pl.pallas_call(
+    return pl.pallas_call(
         functools.partial(kernel, z),
         out_shape=[jax.ShapeDtypeStruct(s, d) for s, d in outs],
         in_specs=[spec] * 8,
@@ -445,6 +939,21 @@
             collective_id=0, has_side_effects=True, vmem_limit_bytes=44 * 2**20
         ),
     )(tokens, cotangent, routes.T, router_expert.T, router_group.T, gate_proj[0], up_proj[0], down_proj[0])
+
+
+def body(axes, tokens, cotangent, routes, router_group, router_expert, gate_proj, up_proj, down_proj):
+    z = sizes_of(axes, tokens, routes, router_group, router_expert, gate_proj)
+    rout_shape = (z.rw, z.ch) if z.reduce_here else (min(z.rw, z.rl), z.width)
+    outs = [
+        ((z.rows, z.cw), BF), ((z.width, z.ff), BF), ((z.width, z.ff), BF), ((z.ff, z.width), BF),
+        ((1, z.width), F32), ((1, z.width), F32), ((1, z.ff), F32), (rout_shape, F32),
+    ]
+    spec = pl.BlockSpec(memory_space=pltpu.VMEM)
+    D = pltpu.SemaphoreType.DMA
+    run = run_sourced if by_source(z) else run_wide
+    tg, gate, up, down, gsq, usq, dsq, rout = run(
+        z, outs, tokens, cotangent, routes, router_group, router_expert, gate_proj, up_proj, down_proj
+    )
     if z.reduce_here:
         half = z.ch // 2
         shapes = [gate, up, down, tg, gsq, usq, dsq]

time: 82.5 us -> 81.5 us (0.988)
  local copies, waits for them, and re-layouts: 7.98 us -> 5.53 us
  Pallas kernels: 73.2 us -> 74.9 us
    unnamed x16 -> x12, local copies, waits for them, and re-layouts: 7.98 us -> 5.53 us
    pallas_call x1, Pallas kernels: 70.8 us -> 72.5 us  [run_sourced(): pl.pallas_call(functools.partial(sourced, z), out_shape=[jax.ShapeDtypeSt...]
where the time goes in v1:
time: 81.5 us; the launch traced here: 81.1 us
  Pallas kernels  74.9 us (92%)
  local copies, waits for them, and re-layouts  5.53 us (7%)
    pallas_call x1, Pallas kernels, run_sourced(): pl.pallas_call(functools.partial(sourced, z), out_shape=[jax.ShapeDtypeSt...  72.5 us
    unnamed x12, local copies, waits for them, and re-layouts  5.53 us
    pallas_call x1, Pallas kernels, body(): pl.pallas_call(functools.partial(finish, z), out_shape=[jax.ShapeDtypeStr...  2.41 us

profile of v1, /device:TPU:0, one launch (start us, length us, event | category | flops | bytes accessed | tf_op | source)
XLA Modules:
  0.0 81.1 jit_solution(13901808464129128997)
XLA Ops:
  0.6 0.0 copy-start.5
  0.7 0.7 copy-done.5
  1.3 0.0 copy-start.1
  1.3 1.0 %copy-done.1 = bf16[128,2048]{1,0:T(8,128)(2,1)S(1)} copy-done((bf16[128,2048]{1,0:T(8,128)(2,1)S(1)}, bf16[128,2048]{1,0:T(8,128)(2,1)}, u32[]{:S(2)}) %copy-start.1) | copy-done | bytes 524312
  2.4 0.0 copy-start.2
  2.4 1.0 %copy-done.2 = bf16[128,2048]{1,0:T(8,128)(2,1)S(1)} copy-done((bf16[128,2048]{1,0:T(8,128)(2,1)S(1)}, bf16[128,2048]{1,0:T(8,128)(2,1)}, u32[]{:S(2)}) %copy-start.2) | copy-done | bytes 524312
  3.4 0.0 copy-start.3
  3.4 0.8 %copy-done.3 = bf16[2048,16]{0,1:T(8,128)(2,1)S(1)} copy-done((bf16[2048,16]{0,1:T(8,128)(2,1)S(1)}, bf16[2048,16]{0,1:T(8,128)(2,1)}, u32[]{:S(2)}) %copy-start.3) | copy-done | bytes 65560
  4.2 0.0 copy-start.4
  4.3 0.7 copy-done.4
  5.0 72.5 %shard_map.159 = (bf16[128,1024]{1,0:T(8,128)(2,1)S(1)}, bf16[2048,256]{1,0:T(8,128)(2,1)S(1)}, bf16[2048,256]{1,0:T(8,128)(2,1)S(1)}, bf16[256,2048]{1,0:T(8,12...) custom-call(bf16[128,2048]{1,0:T(8,128)(2,1)S(1)} %copy-done.1, ...), custom_call_target="tpu_custom_call" | custom-call | tf_op jit(solution)/shard_map/pallas_call | solution.py:888
  77.5 0.0 copy-start
  77.5 1.2 %copy-done = bf16[256,2048]{1,0:T(8,128)(2,1)S(1)} copy-done((bf16[256,2048]{1,0:T(8,128)(2,1)S(1)}, bf16[256,2048]{1,0:T(8,128)(2,1)}, u32[]{:S(2)}) %copy-start) | copy-done | bytes 1048600
  78.7 2.4 %shard_map.160 = (bf16[2048,256]{1,0:T(8,128)(2,1)}, bf16[2048,256]{1,0:T(8,128)(2,1)}, bf16[256,2048]{1,0:T(8,128)(2,1)}, bf16[128,1024]{1,0:T(8,128)(2,1)}, f3...) custom-call(bf16[2048,256]{1,0:T(8,128)(2,1)S(1)} %get-tuple-element, ...), custom_call_target="tpu_custom_call" | custom-call | tf_op jit(solution)/shard_map/pallas_call | solution.py:961
Async XLA Ops:
  0.6 0.7 copy-start.5
  1.3 1.0 %copy-start.1 = (bf16[128,2048]{1,0:T(8,128)(2,1)S(1)}, bf16[128,2048]{1,0:T(8,128)(2,1)}, u32[]{:S(2)}) copy-start(bf16[128,2048]{1,0:T(8,128)(2,1)} %tok_h.1) | copy-start | bytes 1572868
  2.4 1.0 %copy-start.2 = (bf16[128,2048]{1,0:T(8,128)(2,1)S(1)}, bf16[128,2048]{1,0:T(8,128)(2,1)}, u32[]{:S(2)}) copy-start(bf16[128,2048]{1,0:T(8,128)(2,1)} %cot_h.1) | copy-start | bytes 1572868
  3.4 0.8 %copy-start.3 = (bf16[2048,16]{0,1:T(8,128)(2,1)S(1)}, bf16[2048,16]{0,1:T(8,128)(2,1)}, u32[]{:S(2)}) copy-start(bf16[2048,16]{0,1:T(8,128)(2,1)} %param.12) | copy-start | bytes 196612
  4.2 0.7 copy-start.4
  77.5 1.2 %copy-start = (bf16[256,2048]{1,0:T(8,128)(2,1)S(1)}, bf16[256,2048]{1,0:T(8,128)(2,1)}, u32[]{:S(2)}) copy-start(bf16[256,2048]{1,0:T(8,128)(2,1)} %get-tuple-element.30.down_in) | copy-start | bytes 3145732

commit v2 on v0

--- a/solution.py
+++ b/solution.py
@@ -372,39 +372,591 @@
         cp.wait_send()
 
 
+def sourced(
+    z, tok_h, cot_h, routes_h, rexp_h, rgrp_h, gate_h, up_h, down_h,
+    tg_out, gate_out, up_out, down_out, gsq_out, usq_out, dsq_out, rout_out,
+    tok_ref, cot_ref, routes_ref, rexp_ref, rgrp_ref, gate_ref, up_ref, down_ref,
+    rc_ref, s_mat, s_tr, t_mat, t_tr, s1w, r1w, s1, r1, s2m, x2m, s2, x2, y2,
+    gacc, uacc, pacc, gate_tr, up_tr, down_tr,
+    dcat, hid, hid_tr, wp, wpr, pts, ptr, s3m, r3m, s3, r3, s4, r4, dall_ref,
+    sq, sqr, term, tra, tsa, trb,
+    ins, z1s, z1r, p2s, p2r, fs, fr, ws, wr, ptsm, ptrm, r3s, r3r, r4s, r4r, ms, mr, tas, tar, tbs, tbr,
+):
+    e, t = lax.axis_index("ep"), lax.axis_index("tp")
+    g, p = e // z.gs, e % z.gs
+    other = 1 - t
+    hk = [g, g + 1 - 2 * (g % 2), 3 - g, (g + 2) % 4]
+    qd = [p, p + 1 - 2 * (p % 2), (p + 2) % 4, 3 - p]
+    inner = (g + 1) // 2 == 1
+    nj, cc, gr, cap, blk, per = z.nj, z.cc, z.gr, z.cap, z.blk, z.per
+    ng = 2 * nj
+    far = (1, 2, 3)
+
+    def rcopy(src, dst, ss, rs, ep, tp):
+        return pltpu.make_async_remote_copy(
+            src_ref=src, dst_ref=dst, send_sem=ss, recv_sem=rs,
+            device_id=(ep, tp), device_id_type=MESH,
+        )
+
+    barrier = pltpu.get_barrier_semaphore()
+    for k in far:
+        pl.semaphore_signal(barrier, inc=1, device_id=(hk[k] * z.gs + p, t), device_id_type=MESH)
+        pl.semaphore_signal(barrier, inc=1, device_id=(hk[k] * z.gs + p, other), device_id_type=MESH)
+        pl.semaphore_signal(barrier, inc=1, device_id=(g * z.gs + qd[k], t), device_id_type=MESH)
+    pl.semaphore_signal(barrier, inc=1, device_id=(e, other), device_id_type=MESH)
+
+    loads = [
+        pltpu.make_async_copy(a, b, ins.at[i])
+        for i, (a, b) in enumerate((
+            (routes_h, routes_ref), (tok_h, tok_ref), (rexp_h, rexp_ref), (rgrp_h, rgrp_ref),
+            (cot_h, cot_ref), (gate_h, gate_ref), (up_h, up_ref), (down_h, down_ref),
+        ))
+    ]
+    for cp in loads:
+        cp.start()
+
+    def kr(k, n=1):
+        return pl.ds(k * gr, n * gr)
+
+    def kb(k, n=1):
+        return pl.ds(k * blk, n * blk)
+
+    def in_block(k, q):
+        return pl.ds(pl.multiple_of(k * blk + q * cap, cap), cap)
+
+    def three(k):
+        return pl.ds(k * blk, 3 * cap)
+
+    def cols(half, j):
+        return pl.ds(pl.multiple_of(half * z.cw + j * cc, cc), cc)
+
+    def z_copy(src, dst, c, k):
+        return rcopy(src.at[kr(k)], dst.at[kr(k)], z1s.at[c // ng], z1r.at[c, k - 1], hk[k] * z.gs + p, t)
+
+    def spread(src, dst, ss, rs, k):
+        for d in (3, 1, 2):
+            rcopy(src.at[in_block(k, qd[d])], dst.at[in_block(k, p)], ss, rs, g * z.gs + qd[d], t).start()
+        dst[in_block(k, p), :] = src[in_block(k, p), :]
+
+    def gathered(src, dst, ss, rs, k):
+        rcopy(src.at[three(k)], dst.at[three(k)], ss, rs, g * z.gs + qd[3], t).wait_recv()
+
+    def line_out(src, dst, ss, rs, k, line):
+        mine = pl.ds(pl.multiple_of((k * z.gs + p) * 16, 16), 16)
+        src[k * 16 : (k + 1) * 16, :] = line.astype(BF)
+        for d in (3, 1, 2):
+            rcopy(src.at[pl.ds(k * 16, 16)], dst.at[mine], ss, rs, g * z.gs + qd[d], t).start()
+        dst[mine, :] = src[k * 16 : (k + 1) * 16, :]
+
+    def line_wait(dst, ss, rs, k):
+        part = dst.at[pl.ds(k * z.gs * 16, 48)]
+        rcopy(part, part, ss, rs, g * z.gs + qd[3], t).wait_recv()
+
+    def line_column(dst, k):
+        tiles = []
+        for q in range(z.gs):
+            at = (k * z.gs + q) * 16
+            tiles += [dst[at : at + 16, :]] * (cap // 16)
+        rows = jnp.concatenate(tiles, axis=0).astype(F32)
+        r, c = lanes_of((blk, blk), 0), lanes_of((blk, blk), 1)
+        return jnp.sum(jnp.where(c == p * cap + r % cap, rows, 0.0), axis=1, keepdims=True)
+
+    def pair(src, dst, ss, rs):
+        return rcopy(src, dst, ss, rs, e, other)
+
+    lane = lanes_of((z.rows, z.rl))
+    ll, lb = lane % per, lane // per
+    eye = lanes_of((z.rows, z.rows), 0) == lanes_of((z.rows, z.rows), 1)
+
+    def column(row):
+        return jnp.sum(jnp.where(eye, row.astype(F32), 0.0), axis=1, keepdims=True).astype(jnp.int32)
+
+    def before(n):
+        r, c = lanes_of((n, n), 0), lanes_of((n, n), 1)
+        return ((c < r) & (r // gr == c // gr)).astype(F32).astype(BF)
+
+    def make_t(k, n):
+        m = n * gr
+        vals = r1w[kr(k, n), :]
+        member = (vals.astype(F32) > 0.0) & (lanes_of((m, z.rl)) < z.experts)
+        rank = mm(before(m), member.astype(F32).astype(BF))
+        rank = jnp.where(member, rank, -1.0).astype(BF)
+        sr, sc = lanes_of((z.rl, blk), 0) - g * z.gs, lanes_of((z.rl, blk), 1)
+        expand = (sr == sc // cap).astype(F32).astype(BF)
+        spot = (lanes_of((m, blk)) % cap).astype(F32)
+        tf = (mm(rank, expand) == spot).astype(F32)
+        t_mat[kr(k, n), :] = tf.astype(BF)
+        t_tr[:, kr(k, n)] = tf.T.astype(BF)
+
+    def t_rows(k):
+        return t_mat[k * gr : (k + 1) * gr, :]
+
+    def t_cols(k):
+        return t_tr[:, k * gr : (k + 1) * gr]
+
+    loads[0].wait()
+    r0, r1_ = column(routes_ref[0:1, :]), column(routes_ref[1:2, :])
+    chosen = (ll == r0) | (ll == r1_)
+    low = (ll - z.experts) * z.gs
+    is_group = (ll >= z.experts) & (ll < z.experts + z.groups)
+    in_group = is_group & (r0 >= low) & (r0 < low + z.gs)
+    tri = lanes_of((z.rows, z.rows), 1) < lanes_of((z.rows, z.rows), 0)
+    grank = mm(tri.astype(F32).astype(BF), in_group.astype(F32).astype(BF))
+    grank = jnp.where(in_group, grank, -1.0).astype(BF)
+    er, el = lanes_of((z.rl, z.r1), 0) - z.experts, lanes_of((z.rl, z.r1), 1)
+    kk = el // gr
+    want = jnp.where(kk == 0, hk[0], jnp.where(kk == 1, hk[1], jnp.where(kk == 2, hk[2], hk[3])))
+    expand = (er == want).astype(F32).astype(BF)
+    place = (lanes_of((z.rows, z.r1)) % gr).astype(F32)
+    s_f = (mm(grank, expand) == place).astype(F32)
+    s_mat[...] = s_f.astype(BF)
+    s_tr[...] = s_f.T.astype(BF)
+    pick_mask = jnp.where(chosen & (lb == 0), 1.0, 0.0)
+    r1w[kr(0), :] = mm(s_tr[kr(0), :], pick_mask.astype(BF)).astype(BF)
+
+    def fill(c):
+        j = c % nj
+        src = tok_ref if c < nj else cot_ref
+        s1[c] = mm(s_tr[...], src[:, cols(t, j)]).astype(BF)
+        r1[c, kr(0), :] = s1[c, kr(0), :]
+
+    def near_out(c):
+        z_copy(s1.at[c], r1.at[c], c, 1).start()
+
+        @pl.when(inner)
+        def _():
+            z_copy(s1.at[c], r1.at[c], c, 2).start()
+
+    def op_a(k, c):
+        if k:
+            z_copy(s1.at[c], r1.at[c], c, k).wait_recv()
+        s2[c, kb(k), :] = mm(t_cols(k), r1[c, kr(k), :]).astype(BF)
+        spread(s2.at[c], x2.at[c], p2s.at[0], p2r.at[c, k], k)
+
+    def op_am(k):
+        er, ec = lanes_of((z.rl, blk), 0), lanes_of((z.rl, blk), 1)
+        pick = (er == per + g * z.gs + ec // cap).astype(F32).astype(BF)
+        weight = mm(r1w[kr(k), :], pick) * t_rows(k).astype(F32)
+        line_out(s2m, x2m, p2s.at[1], p2r.at[ng, k], k, mm(jnp.ones((16, gr), BF), weight.astype(BF)))
+
+    make_t(0, 1)
+    loads[1].wait()
+    fill(0)
+    pl.semaphore_wait(barrier, 10)
+    near_out(0)
+    op_a(0, 0)
+    for c in range(1, nj):
+        fill(c)
+        near_out(c)
+        op_a(0, c)
+
+    rc_ref[...] = jnp.zeros_like(rc_ref)
+    loads[2].wait()
+    loads[3].wait()
+    for b in range(z.rl // per):
+        rc_ref[b * per : b * per + z.experts, :] = rexp_ref[...]
+        rc_ref[b * per + z.experts : b * per + z.experts + z.groups, :] = rgrp_ref[...]
+    expd = jnp.exp(mm(tok_ref[...], rc_ref[...], 1, 1))
+    gexp = jnp.where(is_group, expd, 0.0)
+    gprob = gexp / jnp.sum(jnp.where(lb == 0, gexp, 0.0), axis=1, keepdims=True)
+    picked = jnp.sum(jnp.where(in_group & (lb == 0), gprob, 0.0), axis=1, keepdims=True)
+    pexp = jnp.where(chosen, expd, 0.0)
+    paired = pexp / jnp.sum(jnp.where(lb == 0, pexp, 0.0), axis=1, keepdims=True)
+    both = paired + gprob
+    upper = both.astype(BF).astype(F32)
+    meta = jnp.where(lb == 1, picked * paired, jnp.where(lb == 2, upper, jnp.where(lb == 3, both - upper, pick_mask)))
+    s1w[...] = mm(s_tr[...], meta.astype(BF)).astype(BF)
+    r1w[kr(0), :] = s1w[kr(0), :]
+    for k in far:
+        z_copy(s1w, r1w, ng, k).start()
+    loads[4].wait()
+    for c in range(nj, ng):
+        fill(c)
+        near_out(c)
+        op_a(0, c)
+
+    def op_s(k):
+        for c in range(ng):
+            z_copy(s1.at[c], r1.at[c], c, k).start()
+
+    @pl.when(inner)
+    def _():
+        op_s(3)
+
+    op_am(0)
+
+    def op_t(k):
+        z_copy(s1w, r1w, ng, k).wait_recv()
+        make_t(k, 1)
+
+    def relay(k, c):
+        return pair(x2.at[c, kb(k)], y2.at[c, kb(k)], fs.at[0], fr.at[c, k])
+
+    def op_b(k, c):
+        gathered(s2.at[c], x2.at[c], p2s.at[0], p2r.at[c, k], k)
+        relay(k, c).start()
+
+    def op_c1(k, n):
+        ga = ua = None
+        for half, xs in ((t, x2), (other, y2)):
+            for j in range(nj):
+                if xs is y2:
+                    for i in range(n):
+                        relay(k + i, j).wait_recv()
+                x, at = xs[j, kb(k, n), :], cols(half, j)
+                a, b = mm(x, gate_ref[at, :]), mm(x, up_ref[at, :])
+                ga, ua = (a, b) if ga is None else (ga + a, ua + b)
+        gacc[kb(k, n), :] = ga
+        uacc[kb(k, n), :] = ua
+
+    def token_term(k, n, half, j):
+        at = cols(half, j)
+        return (
+            mm(dcat[kb(k, n), : z.ff], gate_tr[:, at]) + mm(dcat[kb(k, n), z.ff :], up_tr[:, at])
+        ).astype(BF)
+
+    def w_pair(k, n):
+        return pair(wp.at[kb(k, n)], wpr.at[kb(k, n)], ws.at[0], wr.at[k])
+
+    def pt_pair(j, k, n):
+        return pair(pts.at[j, kb(k, n)], ptr.at[j, kb(k, n)], ptsm.at[0], ptrm.at[j, k])
+
+    def pull(k, n, js, pulled):
+        for half, xs in ((t, x2), (other, y2)):
+            for j in js:
+                if xs is y2:
+                    for i in range(n):
+                        relay(k + i, nj + j).wait_recv()
+                a = mm(xs[nj + j, kb(k, n), :], down_tr[cols(half, j), :])
+                pulled = a if pulled is None else pulled + a
+        return pulled
+
+    def op_p(k, n):
+        pacc[kb(k, n), :] = pull(k, n, range(nj - 1), None)
+
+    def op_c2(k, n):
+        pulled = pull(k, n, (nj - 1,), pacc[kb(k, n), :])
+        for i in range(n):
+            line_wait(x2m, p2s.at[1], p2r.at[ng, k + i], k + i)
+        m = n * blk
+        scale = jnp.concatenate([line_column(x2m, k + i) for i in range(n)], axis=0)
+        gate_pre, up_pre = gacc[kb(k, n), :], uacc[kb(k, n), :]
+        sig = 1.0 / (1.0 + jnp.exp(-gate_pre))
+        silu = gate_pre * sig
+        product = silu * up_pre
+        hidden = product.astype(BF)
+        hid[kb(k, n), :] = (scale * product).astype(BF)
+        wp[kb(k, n), :] = jnp.broadcast_to(
+            jnp.sum(pulled * hidden.astype(F32), axis=1, keepdims=True), (m, z.rl)
+        )
+        w_pair(k, n).start()
+        dh = scale * pulled
+        dcat[kb(k, n), : z.ff] = (dh * up_pre * sig * (1.0 + gate_pre * (1.0 - sig))).astype(BF)
+        dcat[kb(k, n), z.ff :] = (dh * silu).astype(BF)
+        for j in range(nj):
+            pts[j, kb(k, n), :] = token_term(k, n, other, j)
+            pt_pair(j, k, n).start()
+
+    def op_d(k, n, out=False):
+        mine = token_term(k, n, t, 0)
+        w_pair(k, n).wait_recv()
+        wsum = wp[kb(k, n), :] + wpr[kb(k, n), :]
+        same = lanes_of((blk, blk), 0) == lanes_of((blk, blk), 1)
+        for i in range(n):
+            diag = jnp.where(same, wsum[i * blk : (i + 1) * blk, :blk], 0.0).astype(BF)
+            line_out(s3m, r3m, r3s.at[1], r3r.at[nj, k + i], k + i, mm(jnp.ones((16, blk), BF), diag))
+        for j in range(nj):
+            if j:
+                mine = token_term(k, n, t, j)
+            pt_pair(j, k, n).wait_recv()
+            s3[j, kb(k, n), :] = (mine.astype(F32) + ptr[j, kb(k, n), :].astype(F32)).astype(BF)
+            if out:
+                spread(s3.at[j], r3.at[j], r3s.at[0], r3r.at[j, k], k)
+
+    def op_dr(k, n):
+        op_d(k, n, True)
+
+    def op_r(k):
+        for j in range(nj):
+            spread(s3.at[j], r3.at[j], r3s.at[0], r3r.at[j, k], k)
+
+    def home_copy(j, k):
+        return rcopy(s4.at[j, kr(k)], r4.at[j, kr(k)], r4s.at[0], r4r.at[j, k - 1], hk[k] * z.gs + p, t)
+
+    lane3 = lanes_of((gr, z.rl))
+    i1, i2 = lanes_of((z.rl, z.rl), 0), lanes_of((z.rl, z.rl), 1)
+    fold = ((i2 < per) & ((i1 == 2 * per + i2) | (i1 == 3 * per + i2))).astype(F32).astype(BF)
+
+    def op_e(k):
+        vals = mm(r1w[kr(k), :], fold)
+        g_lane = (lane3 >= z.experts) & (lane3 < z.experts + z.groups)
+        pr = jnp.where(lane3 < z.experts, vals, 0.0)
+        here = lane3 == z.experts + g
+        pk = jnp.sum(jnp.where(here, vals, 0.0), axis=1, keepdims=True)
+        line_wait(r3m, r3s.at[1], r3r.at[nj, k], k)
+        lr, lc = lanes_of((blk, z.rl), 0), lanes_of((blk, z.rl), 1)
+        dw = mm(t_rows(k), jnp.where(lc == g * z.gs + lr // cap, line_column(r3m, k), 0.0).astype(BF))
+        dpicked = jnp.sum(dw * pr, axis=1, keepdims=True)
+        q = pk * dw
+        dchosen = pr * (q - jnp.sum(pr * q, axis=1, keepdims=True))
+        dgroup = jnp.where(g_lane, (dpicked * pk) * (here.astype(F32) - vals), 0.0)
+        dall_ref[kr(k), :] = (dchosen + dgroup).astype(BF)
+
+    def op_f(k):
+        dall = dall_ref[kr(k), :]
+        for j in range(nj):
+            gathered(s3.at[j], r3.at[j], r3s.at[0], r3r.at[j, k], k)
+            row = (mm(t_rows(k), r3[j, kb(k), :]) + mm(dall, rc_ref[:, cols(t, j)])).astype(BF)
+            if k:
+                s4[j, kr(k), :] = row
+                home_copy(j, k).start()
+            else:
+                r4[j, kr(k), :] = row
+
+    sub = min(cc, 256)
+    ns = cc // sub
+    ones_ff = jnp.ones((16, z.ff), BF)
+    ones_sub = jnp.ones((16, sub), BF)
+    n_piece = z.cw // sub
+
+    def gate_up_grads(i):
+        half, xs = (t, x2) if i < n_piece else (other, y2)
+        i = i % n_piece
+        j, o = i // ns, (i % ns) * sub
+        at = pl.ds(pl.multiple_of(half * z.cw + i * sub, sub), sub)
+        total = mm(xs[j, :, o : o + sub], dcat[...], 0, 0)
+        gate_out[at, :] = total[:, : z.ff].astype(BF)
+        up_out[at, :] = total[:, z.ff :].astype(BF)
+        square = (total * total).astype(BF)
+        sq[0:1, at] = mm(ones_ff, square[:, : z.ff], 1, 1)[0:1]
+        sq[1:2, at] = mm(ones_ff, square[:, z.ff :], 1, 1)[0:1]
+
+    def down_grads(i):
+        half, xs = (t, x2) if i < n_piece else (other, y2)
+        i = i % n_piece
+        j, o = i // ns, (i % ns) * sub
+        at = pl.ds(pl.multiple_of(half * z.cw + i * sub, sub), sub)
+        total = mm(hid_tr[...], xs[nj + j, :, o : o + sub])
+        down_out[:, at] = total.astype(BF)
+        return mm(ones_sub, (total * total).astype(BF), 1, 1)[0:1]
+
+    loads[5].wait()
+    gate_tr[...] = gate_ref[...].T
+    loads[6].wait()
+    up_tr[...] = up_ref[...].T
+    loads[7].wait()
+    down_tr[...] = down_ref[...].T
+
+    per_core = z.cw // z.ch // z.gs
+    home_core = g // per_core
+    all_a = rcopy(term.at[pl.ds(0, 3)], tra, tas.at[0], tar.at[0], g * z.gs + qd[3], t)
+
+    def term_b(k, core):
+        return rcopy(tsa.at[hk[k] % per_core], trb.at[k], tbs.at[k, core], tbr.at[0], hk[k] * z.gs + p, core)
+
+    t_pair = pair(tsa.at[g % per_core], trb.at[0], ms.at[1], mr.at[1])
+
+    def op_x():
+        dterm = dall_ref[:, : z.rw]
+        for j in range(nj):
+            full = mm(dterm, r1[j], 0, 0)
+            for i in range(cc // z.ch):
+                n = j * (cc // z.ch) + i
+                term[n % z.gs, n // z.gs] = full[:, i * z.ch : (i + 1) * z.ch]
+        for d in far:
+            rcopy(term.at[qd[d]], tra.at[d - 1], tas.at[0], tar.at[0], g * z.gs + qd[d], t).start()
+
+    def op_y():
+        all_a.wait_recv()
+        tsa[...] = term[p] + tra[0] + tra[1] + tra[2]
+        for k in far:
+
+            @pl.when(hk[k] // per_core == t)
+            def _():
+                for core in range(z.n_tp):
+                    term_b(k, core).start()
+
+        @pl.when(home_core == t)
+        def _():
+            t_pair.start()
+
+    sq_copy = pair(sq, sqr, ms.at[0], mr.at[0])
+
+    def op_h():
+        hid_tr[...] = hid[...].T
+
+    def op_q():
+        sq_copy.start()
+
+    def op_w(i):
+        part = down_grads(i)
+        dsq_out[...] = dsq_out[...] + part if i else part
+
+    ops = {
+        "t": op_t, "a": op_a, "m": op_am, "b": op_b, "c": op_c1, "p": op_p, "C": op_c2, "d": op_d, "D": op_dr, "r": op_r,
+        "e": op_e, "f": op_f, "x": op_x, "y": op_y, "g": gate_up_grads, "h": op_h, "q": op_q, "w": op_w, "s": op_s,
+    }
+
+    def play(text):
+        for word in " ".join(text).split():
+            ops[word[0]](*(int(x) for x in word[1:]))
+
+    @pl.when((g + 1) // 2 != 1)
+    def _():
+        play(z.order_end)
+
+    @pl.when(inner)
+    def _():
+        play(z.order_mid)
+
+    def home(j):
+        for k in far:
+            home_copy(j, k).wait_recv()
+        tg_out[:, j * cc : (j + 1) * cc] = mm(s_mat[...], r4[j]).astype(BF)
+
+    for j in range(nj):
+        home(j)
+    sq_copy.wait_recv()
+    gsq_out[...] = sq[0:1, :] + sqr[0:1, :]
+    usq_out[...] = sq[1:2, :] + sqr[1:2, :]
+    got = trb.at[pl.ds(1, 3)]
+    rcopy(got, got, tbs.at[1, 0], tbr.at[0], e, other).wait_recv()
+
+    @pl.when(home_core == t)
+    def _():
+        rout_out[...] = tsa[g % per_core] + trb[1] + trb[2] + trb[3]
+
+    @pl.when(home_core != t)
+    def _():
+        t_pair.wait_recv()
+        rout_out[...] = trb[0] + trb[1] + trb[2] + trb[3]
+
+    @pl.when(home_core == t)
+    def _():
+        t_pair.wait_send()
+
+    for k in far:
+
+        @pl.when(hk[k] // per_core == t)
+        def _():
+            for core in range(z.n_tp):
+                term_b(k, core).wait_send()
+
+    most, some = pl.ds(0, 3 * blk), pl.ds(0, 16 * 12)
+
+    def left(src, dst, ss, rs):
+        rcopy(src, dst, ss, rs, e, other).wait_send()
+
+    left(s1.at[:, kr(1, 3)], r1.at[:, kr(1, 3)], z1s.at[0], z1r.at[0, 0])
+    left(s1w.at[kr(1, 3)], r1w.at[kr(1, 3)], z1s.at[1], z1r.at[ng, 0])
+    left(s2.at[:, most], x2.at[:, most], p2s.at[0], p2r.at[0, 0])
+    left(x2m.at[some], x2m.at[some], p2s.at[1], p2r.at[ng, 0])
+    left(x2, y2, fs.at[0], fr.at[0, 0])
+    left(wp, wpr, ws.at[0], wr.at[0])
+    left(pts, ptr, ptsm.at[0], ptrm.at[0, 0])
+    left(s3.at[:, most], r3.at[:, most], r3s.at[0], r3r.at[0, 0])
+    left(r3m.at[some], r3m.at[some], r3s.at[1], r3r.at[nj, 0])
+    left(s4.at[:, kr(1, 3)], r4.at[:, kr(1, 3)], r4s.at[0], r4r.at[0, 0])
+    all_a.wait_send()
+    sq_copy.wait_send()
+
+
 def finish(
     z, gate_in, up_in, down_in, tg_in, gsq_in, usq_in, dsq_in, rout_in,
-    gate_out, up_out, down_out, tg_out, gsq_out, usq_out, dsq_out, reg_out, rgg_out, rows_out, sem,
+    gate_out, up_out, down_out, tg_out, gsq_out, usq_out, dsq_out, reg_out, rgg_out, rows_out,
+    reg_ref, rgg_ref, rows_ref, sem,
 ):
-    copies = []
-    pairs = (
+    pairs = [
         (gate_in, gate_out), (up_in, up_out), (down_in, down_out), (tg_in, tg_out),
         (gsq_in, gsq_out), (usq_in, usq_out), (dsq_in, dsq_out),
-    )
-    for i, (src, dst) in enumerate(pairs):
-        cp = pltpu.make_async_copy(src, dst, sem.at[i])
+        (reg_ref, reg_out), (rgg_ref, rgg_out), (rows_ref, rows_out),
+    ]
+    copies = [pltpu.make_async_copy(src, dst, sem.at[i]) for i, (src, dst) in enumerate(pairs)]
+    for cp in copies[:7]:
         cp.start()
-        copies.append(cp)
     half = z.ch // 2
     both = rout_in[...]
     mine = jnp.where(lax.axis_index("tp") == 0, both[:, :half], both[:, half:])
     reg = mine[: z.experts]
     rgg = mine[z.experts : z.experts + z.groups]
-    reg_out[...] = reg
-    rgg_out[...] = rgg
-    rows_out[...] = jnp.sum(reg * reg, axis=0, keepdims=True) + jnp.sum(rgg * rgg, axis=0, keepdims=True)
+    reg_ref[...] = reg
+    rgg_ref[...] = rgg
+    rows_ref[...] = jnp.sum(reg * reg, axis=0, keepdims=True) + jnp.sum(rgg * rgg, axis=0, keepdims=True)
+    for cp in copies[7:]:
+        cp.start()
     for cp in copies:
         cp.wait()
 
 
-def body(axes, tokens, cotangent, routes, router_group, router_expert, gate_proj, up_proj, down_proj):
-    z = sizes_of(axes, tokens, routes, router_group, router_expert, gate_proj)
+def by_source(z):
+    return (
+        z.reduce_here and z.groups == 4 and z.gs == 4 and z.cap % 16 == 0 and z.gr % 16 == 0
+        and z.experts + z.groups <= z.rl // 4 and z.cw % 512 == 0 and (z.cw // z.ch) % z.gs == 0
+    )
+
+
+def run_sourced(z, outs, tokens, cotangent, routes, router_group, router_expert, gate_proj, up_proj, down_proj):
+    z.nj = 2
+    z.cc = z.cw // z.nj
+    z.blk = z.gs * z.cap
+    z.per = z.rl // 4
+    z.order_end = (
+        "t1 a10 b00 a11", "b01 a12 b02 a13", "b03 m1 b10 t3", "a30 b11 a31 b12", "a32 s2 s3 b13",
+        "a33 m3 c02 p02", "C02 d02 t2 a20", "b30 b31 a21 c31", "a22 b32 p31 b33", "a23 m2 C31 b20",
+        "b21 D31 r1 c21", "b22 p21 b23 C21", "D21 e3 f3 e1", "e0 g0 e2 x", "r0 f2 f1 g1", "g2 y g3 g4",
+        "g5 g6 g7 q", "h w0 w1 f0", "w2 w3 w4 w5", "w6 w7",
+    )
+    z.order_mid = (
+        "t1 a10 b00 a11", "b01 a12 b02 a13", "b03 m1 t2 a20", "a21 a22 a23 m2", "b10 b11 c02 b12",
+        "p02 b13 C02 d02", "r1 b20 b21 c21", "b22 p21 b23 t3", "a30 a31 C21 a32", "a33 m3 D21 e0",
+        "e1 f1 b30 b31", "c31 b32 p31 b33", "C31 e2 f2 D31", "g0 g1 g2 g3", "e3 x r0 f3", "g4 g5 g6 g7",
+        "q h y w0", "w1 w2 f0 w3", "w4 w5 w6 w7",
+    )
+    nj, ng, cc = z.nj, 2 * z.nj, z.cc
+    V = pltpu.VMEM
+    args = (tokens, cotangent, routes.T, router_expert.T, router_group.T, gate_proj[0], up_proj[0], down_proj[0])
+    hb = z.cw // z.ch // z.gs
+    scratch = [V(a.shape, a.dtype) for a in args] + [
+        V((z.rl, z.width), BF), V((z.rows, z.r1), BF), V((z.r1, z.rows), BF),
+        V((z.r1, z.blk), BF), V((z.blk, z.r1), BF),
+        V((z.r1, z.rl), BF), V((z.r1, z.rl), BF),
+        V((ng, z.r1, cc), BF), V((ng, z.r1, cc), BF),
+        V((16 * 4, z.blk), BF), V((16 * 4 * z.gs, z.blk), BF),
+        V((ng, z.pairs, cc), BF), V((ng, z.pairs, cc), BF), V((ng, z.pairs, cc), BF),
+        V((z.pairs, z.ff), F32), V((z.pairs, z.ff), F32), V((z.pairs, z.ff), F32),
+        V((z.ff, z.width), BF), V((z.ff, z.width), BF), V((z.width, z.ff), BF),
+        V((z.pairs, 2 * z.ff), BF), V((z.pairs, z.ff), BF), V((z.ff, z.pairs), BF),
+        V((z.pairs, z.rl), F32), V((z.pairs, z.rl), F32),
+        V((nj, z.pairs, cc), BF), V((nj, z.pairs, cc), BF),
+        V((16 * 4, z.blk), BF), V((16 * 4 * z.gs, z.blk), BF),
+        V((nj, z.pairs, cc), BF), V((nj, z.pairs, cc), BF),
+        V((nj, z.r1, cc), BF), V((nj, z.r1, cc), BF), V((z.r1, z.rl), BF),
+        V((2, z.width), F32), V((2, z.width), F32),
+        V((z.gs, hb, z.rw, z.ch), F32), V((z.gs - 1, hb, z.rw, z.ch), F32), V((hb, z.rw, z.ch), F32),
+        V((z.groups, z.rw, z.ch), F32),
+    ]
+    D = pltpu.SemaphoreType.DMA
+    sems = [D((len(args),))] + [
+        D(s) for s in (
+            (2,), (ng + 1, 3), (2,), (ng + 1, 4), (1,), (ng, 4), (1,), (4,), (1,), (nj, 4),
+            (2,), (nj + 1, 4), (1,), (nj, 3), (2,), (2,), (1,), (1,), (4, 2), (1,),
+        )
+    ]
+    spec = pl.BlockSpec(memory_space=pltpu.VMEM)
+    return pl.pallas_call(
+        functools.partial(sourced, z),
+        out_shape=[pltpu.VMEM(s, d) for s, d in outs],
+        in_specs=[pl.BlockSpec(memory_space=pltpu.HBM)] * len(args),
+        out_specs=[spec] * len(outs),
+        scratch_shapes=scratch + sems,
+        compiler_params=pltpu.CompilerParams(
+            collective_id=0, has_side_effects=True, vmem_limit_bytes=44 * 2**20
+        ),
+    )(*[pltpu.with_memory_space_constraint(a, pltpu.HBM) for a in args])
+
+
+def run_wide(z, outs, tokens, cotangent, routes, router_group, router_expert, gate_proj, up_proj, down_proj):
     h, nc, cc = z.half_chunks, z.nc, z.cc
-    rout_shape = (z.rw, z.ch) if z.reduce_here else (min(z.rw, z.rl), z.width)
-    outs = [
-        ((z.rows, z.cw), BF), ((z.width, z.ff), BF), ((z.width, z.ff), BF), ((z.ff, z.width), BF),
-        ((1, z.width), F32), ((1, z.width), F32), ((1, z.ff), F32), (rout_shape, F32),
-    ]
     V = pltpu.VMEM
     chd = z.ch if z.reduce_here else 128
     scratch = [
@@ -435,7 +987,7 @@
         D((3,)), D((3,)), D((z.n_ep // 2,)), D((z.n_ep // 2,)),
     ]
     spec = pl.BlockSpec(memory_space=pltpu.VMEM)
-    tg, gate, up, down, gsq, usq, dsq, rout = pl.pallas_call(
+    return pl.pallas_call(
         functools.partial(kernel, z),
         out_shape=[jax.ShapeDtypeStruct(s, d) for s, d in outs],
         in_specs=[spec] * 8,
@@ -445,6 +997,21 @@
             collective_id=0, has_side_effects=True, vmem_limit_bytes=44 * 2**20
         ),
     )(tokens, cotangent, routes.T, router_expert.T, router_group.T, gate_proj[0], up_proj[0], down_proj[0])
+
+
+def body(axes, tokens, cotangent, routes, router_group, router_expert, gate_proj, up_proj, down_proj):
+    z = sizes_of(axes, tokens, routes, router_group, router_expert, gate_proj)
+    rout_shape = (z.rw, z.ch) if z.reduce_here else (min(z.rw, z.rl), z.width)
+    outs = [
+        ((z.rows, z.cw), BF), ((z.width, z.ff), BF), ((z.width, z.ff), BF), ((z.ff, z.width), BF),
+        ((1, z.width), F32), ((1, z.width), F32), ((1, z.ff), F32), (rout_shape, F32),
+    ]
+    spec = pl.BlockSpec(memory_space=pltpu.VMEM)
+    D = pltpu.SemaphoreType.DMA
+    run = run_sourced if by_source(z) else run_wide
+    tg, gate, up, down, gsq, usq, dsq, rout = run(
+        z, outs, tokens, cotangent, routes, router_group, router_expert, gate_proj, up_proj, down_proj
+    )
     if z.reduce_here:
         half = z.ch // 2
         shapes = [gate, up, down, tg, gsq, usq, dsq]
@@ -454,8 +1021,8 @@
             out_shape=[jax.ShapeDtypeStruct(a.shape, a.dtype) for a in shapes]
             + [jax.ShapeDtypeStruct((n, half), F32) for n in (z.experts, z.groups, 1)],
             in_specs=[spec] * 8,
-            out_specs=[anywhere] * 7 + [spec] * 3,
-            scratch_shapes=[D((7,))],
+            out_specs=[anywhere] * 10,
+            scratch_shapes=[pltpu.VMEM((n, half), F32) for n in (z.experts, z.groups, 1)] + [D((10,))],
             compiler_params=pltpu.CompilerParams(vmem_limit_bytes=16 * 2**20),
         )(*shapes, rout)
         reg, rgg, rrows = reg.T, rgg.T, rrows[0]

time: 82.5 us -> 56 us (0.68)
  Pallas kernels: 73.2 us -> 55 us
  local copies, waits for them, and re-layouts: 7.98 us -> 0 us
    pallas_call x1, Pallas kernels: 70.8 us -> 53.2 us  [run_sourced(): pl.pallas_call(functools.partial(sourced, z), out_shape=[pltpu.VMEM(s, d)...]
    unnamed x16 -> x0, local copies, waits for them, and re-layouts: 7.98 us -> none
where the time goes in v2:
time: 56 us; the launch traced here: 55.8 us
  Pallas kernels  55 us (98%)
  between operations  0.81 us (1%)
    pallas_call x1, Pallas kernels, run_sourced(): pl.pallas_call(functools.partial(sourced, z), out_shape=[pltpu.VMEM(s, d)...  53.2 us
    pallas_call x1, Pallas kernels, body(): pl.pallas_call(functools.partial(finish, z), out_shape=[jax.ShapeDtypeStr...  1.84 us

profile of v2, /device:TPU:0, one launch (start us, length us, event | category | flops | bytes accessed | tf_op | source)
XLA Modules:
  0.0 55.8 jit_solution(7817557945556194881)
XLA Ops:
  0.6 53.2 %shard_map.159 = (bf16[128,1024]{1,0:T(8,128)(2,1)S(1)}, bf16[2048,256]{1,0:T(8,128)(2,1)S(1)}, bf16[2048,256]{1,0:T(8,128)(2,1)S(1)}, bf16[256,2048]{1,0:T(8,12...) custom-call(bf16[128,2048]{1,0:T(8,128)(2,1)} %tok_h.1, ...), custom_call_target="tpu_custom_call" | custom-call | tf_op jit(solution)/shard_map/pallas_call | solution.py:946
  53.8 1.8 %shard_map.160 = (bf16[2048,256]{1,0:T(8,128)(2,1)}, bf16[2048,256]{1,0:T(8,128)(2,1)}, bf16[256,2048]{1,0:T(8,128)(2,1)}, bf16[128,1024]{1,0:T(8,128)(2,1)}, f3...) custom-call(bf16[2048,256]{1,0:T(8,128)(2,1)S(1)} %get-tuple-element, ...), custom_call_target="tpu_custom_call" | custom-call | tf_op jit(solution)/shard_map/pallas_call | solution.py:1019

commit v3 on v2

--- a/solution.py
+++ b/solution.py
@@ -590,7 +590,7 @@
         make_t(k, 1)
 
     def relay(k, c):
-        return pair(x2.at[c, kb(k)], y2.at[c, kb(k)], fs.at[0], fr.at[c, k])
+        return pair(x2.at[c, kb(k)], y2.at[c, kb(k)], fs.at[0], fr.at[max(0, c - nj + 1), k])
 
     def op_b(k, c):
         gathered(s2.at[c], x2.at[c], p2s.at[0], p2r.at[c, k], k)
@@ -600,9 +600,10 @@
         ga = ua = None
         for half, xs in ((t, x2), (other, y2)):
             for j in range(nj):
-                if xs is y2:
+                if xs is y2 and j == 0:
                     for i in range(n):
-                        relay(k + i, j).wait_recv()
+                        both_in = pl.ds(0, nj), kb(k + i)
+                        pair(x2.at[both_in], y2.at[both_in], fs.at[0], fr.at[0, k + i]).wait_recv()
                 x, at = xs[j, kb(k, n), :], cols(half, j)
                 a, b = mm(x, gate_ref[at, :]), mm(x, up_ref[at, :])
                 ga, ua = (a, b) if ga is None else (ga + a, ua + b)
@@ -681,7 +682,7 @@
             spread(s3.at[j], r3.at[j], r3s.at[0], r3r.at[j, k], k)
 
     def home_copy(j, k):
-        return rcopy(s4.at[j, kr(k)], r4.at[j, kr(k)], r4s.at[0], r4r.at[j, k - 1], hk[k] * z.gs + p, t)
+        return rcopy(s4.at[j, kr(k)], r4.at[j, kr(k)], r4s.at[0], r4r.at[j], hk[k] * z.gs + p, t)
 
     lane3 = lanes_of((gr, z.rl))
     i1, i2 = lanes_of((z.rl, z.rl), 0), lanes_of((z.rl, z.rl), 1)
@@ -752,7 +753,7 @@
     all_a = rcopy(term.at[pl.ds(0, 3)], tra, tas.at[0], tar.at[0], g * z.gs + qd[3], t)
 
     def term_b(k, core):
-        return rcopy(tsa.at[hk[k] % per_core], trb.at[k], tbs.at[k, core], tbr.at[0], hk[k] * z.gs + p, core)
+        return rcopy(tsa.at[hk[k] % per_core], trb.at[k], tbs.at[0], tbr.at[0], hk[k] * z.gs + p, core)
 
     t_pair = pair(tsa.at[g % per_core], trb.at[0], ms.at[1], mr.at[1])
 
@@ -810,8 +811,7 @@
         play(z.order_mid)
 
     def home(j):
-        for k in far:
-            home_copy(j, k).wait_recv()
+        rcopy(s4.at[j, kr(1, 3)], r4.at[j, kr(1, 3)], r4s.at[0], r4r.at[j], e, other).wait_recv()
         tg_out[:, j * cc : (j + 1) * cc] = mm(s_mat[...], r4[j]).astype(BF)
 
     for j in range(nj):
@@ -820,7 +820,7 @@
     gsq_out[...] = sq[0:1, :] + sqr[0:1, :]
     usq_out[...] = sq[1:2, :] + sqr[1:2, :]
     got = trb.at[pl.ds(1, 3)]
-    rcopy(got, got, tbs.at[1, 0], tbr.at[0], e, other).wait_recv()
+    rcopy(got, got, tbs.at[0], tbr.at[0], e, other).wait_recv()
 
     @pl.when(home_core == t)
     def _():
@@ -834,13 +834,11 @@
     @pl.when(home_core == t)
     def _():
         t_pair.wait_send()
-
-    for k in far:
-
-        @pl.when(hk[k] // per_core == t)
-        def _():
-            for core in range(z.n_tp):
-                term_b(k, core).wait_send()
+        rcopy(trb.at[pl.ds(0, 2)], trb.at[pl.ds(0, 2)], tbs.at[0], tbr.at[0], e, other).wait_send()
+
+    @pl.when(home_core != t)
+    def _():
+        rcopy(trb, trb, tbs.at[0], tbr.at[0], e, other).wait_send()
 
     most, some = pl.ds(0, 3 * blk), pl.ds(0, 16 * 12)
 
@@ -856,7 +854,7 @@
     left(pts, ptr, ptsm.at[0], ptrm.at[0, 0])
     left(s3.at[:, most], r3.at[:, most], r3s.at[0], r3r.at[0, 0])
     left(r3m.at[some], r3m.at[some], r3s.at[1], r3r.at[nj, 0])
-    left(s4.at[:, kr(1, 3)], r4.at[:, kr(1, 3)], r4s.at[0], r4r.at[0, 0])
+    left(s4.at[:, kr(1, 3)], r4.at[:, kr(1, 3)], r4s.at[0], r4r.at[0])
     all_a.wait_send()
     sq_copy.wait_send()
 
@@ -938,8 +936,8 @@
     D = pltpu.SemaphoreType.DMA
     sems = [D((len(args),))] + [
         D(s) for s in (
-            (2,), (ng + 1, 3), (2,), (ng + 1, 4), (1,), (ng, 4), (1,), (4,), (1,), (nj, 4),
-            (2,), (nj + 1, 4), (1,), (nj, 3), (2,), (2,), (1,), (1,), (4, 2), (1,),
+            (2,), (ng + 1, 3), (2,), (ng + 1, 4), (1,), (nj + 1, 4), (1,), (4,), (1,), (nj, 4),
+            (2,), (nj + 1, 4), (1,), (nj,), (2,), (2,), (1,), (1,), (1,), (1,),
         )
     ]
     spec = pl.BlockSpec(memory_space=pltpu.VMEM)

time: 56 us -> 55.8 us (level)
  no operation moved by 1% of the time
where the time goes in v3:
time: 55.8 us; the launch traced here: 55.6 us
  Pallas kernels  54.8 us (98%)
  between operations  0.81 us (1%)
    pallas_call x1, Pallas kernels, run_sourced(): pl.pallas_call(functools.partial(sourced, z), out_shape=[pltpu.VMEM(s, d)...  53 us
    pallas_call x1, Pallas kernels, body(): pl.pallas_call(functools.partial(finish, z), out_shape=[jax.ShapeDtypeStr...  1.84 us

profile of v3, /device:TPU:0, one launch (start us, length us, event | category | flops | bytes accessed | tf_op | source)
XLA Modules:
  0.0 55.6 jit_solution(9310275832798443085)
XLA Ops:
  0.6 53.0 %shard_map.159 = (bf16[128,1024]{1,0:T(8,128)(2,1)S(1)}, bf16[2048,256]{1,0:T(8,128)(2,1)S(1)}, bf16[2048,256]{1,0:T(8,128)(2,1)S(1)}, bf16[256,2048]{1,0:T(8,12...) custom-call(bf16[128,2048]{1,0:T(8,128)(2,1)} %tok_h.1, ...), custom_call_target="tpu_custom_call" | custom-call | tf_op jit(solution)/shard_map/pallas_call | solution.py:944
  53.6 1.8 %shard_map.160 = (bf16[2048,256]{1,0:T(8,128)(2,1)}, bf16[2048,256]{1,0:T(8,128)(2,1)}, bf16[256,2048]{1,0:T(8,128)(2,1)}, bf16[128,1024]{1,0:T(8,128)(2,1)}, f3...) custom-call(bf16[2048,256]{1,0:T(8,128)(2,1)S(1)} %get-tuple-element, ...), custom_call_target="tpu_custom_call" | custom-call | tf_op jit(solution)/shard_map/pallas_call | solution.py:1017

commit v4 on v3

--- a/solution.py
+++ b/solution.py
@@ -900,14 +900,14 @@
     z.per = z.rl // 4
     z.order_end = (
         "t1 a10 b00 a11", "b01 a12 b02 a13", "b03 m1 b10 t3", "a30 b11 a31 b12", "a32 s2 s3 b13",
-        "a33 m3 c02 p02", "C02 d02 t2 a20", "b30 b31 a21 c31", "a22 b32 p31 b33", "a23 m2 C31 b20",
-        "b21 D31 r1 c21", "b22 p21 b23 C21", "D21 e3 f3 e1", "e0 g0 e2 x", "r0 f2 f1 g1", "g2 y g3 g4",
+        "a33 m3 c02 p02", "C02 d02 t2 a20", "b30 b31 a21 b32", "c31 b33 a22 p31", "C31 a23 m2 b20",
+        "D31 b21 r1 c21", "b22 b23 p21 e3", "C21 D21 f3 e1", "e0 g0 e2 x", "r0 f2 f1 g1", "g2 y g3 g4",
         "g5 g6 g7 q", "h w0 w1 f0", "w2 w3 w4 w5", "w6 w7",
     )
     z.order_mid = (
         "t1 a10 b00 a11", "b01 a12 b02 a13", "b03 m1 t2 a20", "a21 a22 a23 m2", "b10 b11 c02 b12",
-        "p02 b13 C02 d02", "r1 b20 b21 c21", "b22 p21 b23 t3", "a30 a31 C21 a32", "a33 m3 D21 e0",
-        "e1 f1 b30 b31", "c31 b32 p31 b33", "C31 e2 f2 D31", "g0 g1 g2 g3", "e3 x r0 f3", "g4 g5 g6 g7",
+        "b13 p02 C02 d02", "r1 b20 b21 c21", "b22 b23 p21 t3", "a30 a31 C21 a32", "a33 m3 D21 e0",
+        "e1 f1 b30 b31", "c31 b32 b33 p31", "C31 e2 f2 D31", "g0 g1 g2 e3", "x r0 f3 g3", "g4 g5 g6 g7",
         "q h y w0", "w1 w2 f0 w3", "w4 w5 w6 w7",
     )
     nj, ng, cc = z.nj, 2 * z.nj, z.cc

time: 55.8 us -> 55.5 us (level)
  no operation moved by 1% of the time
where the time goes in v4:
time: 55.5 us; the launch traced here: 55.3 us
  Pallas kernels  54.5 us (98%)
  between operations  0.81 us (1%)
    pallas_call x1, Pallas kernels, run_sourced(): pl.pallas_call(functools.partial(sourced, z), out_shape=[pltpu.VMEM(s, d)...  52.7 us
    pallas_call x1, Pallas kernels, body(): pl.pallas_call(functools.partial(finish, z), out_shape=[jax.ShapeDtypeStr...  1.84 us

profile of v4, /device:TPU:0, one launch (start us, length us, event | category | flops | bytes accessed | tf_op | source)
XLA Modules:
  0.0 55.3 jit_solution(2025356360447998448)
XLA Ops:
  0.6 52.7 %shard_map.159 = (bf16[128,1024]{1,0:T(8,128)(2,1)S(1)}, bf16[2048,256]{1,0:T(8,128)(2,1)S(1)}, bf16[2048,256]{1,0:T(8,128)(2,1)S(1)}, bf16[256,2048]{1,0:T(8,12...) custom-call(bf16[128,2048]{1,0:T(8,128)(2,1)} %tok_h.1, ...), custom_call_target="tpu_custom_call" | custom-call | tf_op jit(solution)/shard_map/pallas_call | solution.py:944
  53.3 1.8 %shard_map.160 = (bf16[2048,256]{1,0:T(8,128)(2,1)}, bf16[2048,256]{1,0:T(8,128)(2,1)}, bf16[256,2048]{1,0:T(8,128)(2,1)}, bf16[128,1024]{1,0:T(8,128)(2,1)}, f3...) custom-call(bf16[2048,256]{1,0:T(8,128)(2,1)S(1)} %get-tuple-element, ...), custom_call_target="tpu_custom_call" | custom-call | tf_op jit(solution)/shard_map/pallas_call | solution.py:1017
